TPU v7x, 256 devices: a whole 4x4x8 slice. The times are simulated.
256 devices in a mesh: fs: 32 (over z, x), rep: 4 (over y), tp: 2 (over core).
Axes of the slice: x: 4, y: 4, z: 8, core: 2. Of those that a mesh axis runs over, the one named last changes fastest.
Arguments:
- saved_input: bfloat16 [131072, 2048], P(('fs', 'rep')), may hold values from -500 to 500
- query_cotangent: bfloat16 [131072, 2048], P(('fs', 'rep'), 'tp'), may hold values from -0.0049438477 to 0.0049438477
- key_cotangent: bfloat16 [131072, 512], P(('fs', 'rep'), 'tp'), may hold values from -0.0049438477 to 0.0049438477
- query_weight: float32 [2048, 2048], P('fs', 'tp'), may hold values from -45 to 45
- key_weight: float32 [2048, 512], P('fs', 'tp'), may hold values from -45 to 45
- query_moment: float32 [2048, 2048], P('fs', 'tp'), may hold values from -45 to 45
- key_moment: float32 [2048, 512], P('fs', 'tp'), may hold values from -45 to 45
- query_row_root: bfloat16 [2048, 2048], P('fs'), may hold values from -1 to 3, as said below
- key_row_root: bfloat16 [2048, 2048], P('fs'), may hold values from -1 to 3, as said below
- query_head_root: bfloat16 [32, 64, 64], P('tp'), may hold values from -1 to 3, as said below
- key_head_root: bfloat16 [8, 64, 64], P('tp'), may hold values from -1 to 3, as said below
- query_head_stat: float32 [32, 64, 64], P('tp'), may hold values from -26 to 27, as said below
- key_head_stat: float32 [8, 64, 64], P('tp'), may hold values from -26 to 27, as said below
Outputs:
- query_step: float32 [2048, 2048], P('fs', 'tp')
- key_step: float32 [2048, 512], P('fs', 'tp')
- query_next: float32 [2048, 2048], P('fs', 'tp')
- key_next: float32 [2048, 512], P('fs', 'tp')
- query_copy: bfloat16 [2048, 2048], P(None, 'tp')
- key_copy: bfloat16 [2048, 512], P(None, 'tp')
- query_moment_next: float32 [2048, 2048], P('fs', 'tp')
- key_moment_next: float32 [2048, 512], P('fs', 'tp')
- query_stat_next: float32 [32, 64, 64], P('tp')
- key_stat_next: float32 [8, 64, 64], P('tp')
Inputs may be any that keep to these rules, and one draw needn't show every extreme that they name: `query_row_root`: symmetric. `key_row_root`: symmetric. `query_head_root`: each head's matrix is symmetric. `key_head_root`: each head's matrix is symmetric. `query_head_stat`: each head's matrix is symmetric. `key_head_stat`: each head's matrix is symmetric.
All inputs are finite; a program needn't handle non-finite values.
Results may differ from a plain program's by a relative error of at most 0.0018.
The roundings to bfloat16 on the way count: a program that leaves them out, or rounds other values in their place, can miss the bound.
Values may be sent and summed in bfloat16 or wider, within the bound.
A program may use at most 128 MiB of HBM per device.

v0:
```python
import jax
import jax.numpy as jnp
from jax import lax
from jax.sharding import Mesh
from jax.sharding import PartitionSpec as P

D = 2048
HEAD_DIM = 64
FS = ("fs_0", "fs_1")
FS_TP = ("fs_0", "fs_1", "tp")
FS_REP = ("fs_0", "fs_1", "rep")


MOMENT_DECAY = 0.8
STAT_DECAY = 0.5
LEARN_RATE = 0.1
EPSILON = 1e-06


def sum_by_axis(total, axes):
    for axis in axes:
        total = lax.psum_scatter(total, axis, scatter_dimension=0, tiled=True)
    return total


def copy_for_each(value, axis):
    count = lax.axis_size(axis)
    return lax.all_to_all(
        jnp.broadcast_to(value[None], (count, *value.shape)), axis, 0, 0, tiled=True
    )


def of_everyone(value, axis):
    return copy_for_each(value, axis).sum(axis=0)


def in_blocks(value, dim, count):
    dims = value.shape
    parts = value.reshape(*dims[:dim], count, dims[dim] // count, *dims[dim + 1 :])
    return jnp.moveaxis(parts, dim, 0)


def sum_at_owner(value, axis, dim):
    parts = in_blocks(value, dim, lax.axis_size(axis))
    arrived = lax.all_to_all(parts, axis, split_axis=0, concat_axis=0, tiled=True)
    return arrived.sum(axis=0)


def filled_up(lines, count):
    spare = -lines.shape[0] % count
    if not spare:
        return lines
    return jnp.concatenate([lines, jnp.zeros((spare, *lines.shape[1:]), lines.dtype)])


def laid_out(parts, dim):
    parts = jnp.moveaxis(parts, 0, dim)
    dims = parts.shape
    return parts.reshape(*dims[:dim], dims[dim] * dims[dim + 1], *dims[dim + 2 :])


def gathered_copies(value, axis, dim):
    parts = copy_for_each(value, axis)
    return laid_out(parts, dim)


def total_of(value, axes):
    own = sum_at_owner(filled_up(value, lax.axis_size(axes)), axes, 0)
    whole = gathered_copies(own, axes, 0)
    return whole[: len(value)].reshape(value.shape)


def in_one(arrays, axis):
    flat, at, done = (jnp.concatenate([a.reshape(-1) for a in arrays]), 0, [])
    total = total_of(flat, axis)
    for a in arrays:
        done.append(total[at : at + a.size].reshape(a.shape))
        at += a.size
    return tuple(done)


def side_by_side(arrays, axis, dim, along):
    ends, at = ([], 0)
    for a in arrays[:-1]:
        at += a.shape[along]
        ends.append(at)
    both = jnp.concatenate(arrays, axis=along)
    return tuple(jnp.split(lax.all_gather(both, axis, axis=dim, tiled=True), ends, axis=along))


def in_one_2(arrays, axis):
    ends = [0]
    for a in arrays:
        ends.append(ends[-1] + a.size)
    total = of_everyone(jnp.concatenate([a.ravel() for a in arrays]), axis)
    return tuple((total[b:e].reshape(a.shape) for a, b, e in zip(arrays, ends, ends[1:])))


def head_gram(rounded, head_count):
    shaped = rounded.reshape(rounded.shape[0], head_count, HEAD_DIM)
    return jnp.einsum("rhd,rhe->hde", shaped, shaped, preferred_element_type=jnp.float32)


def column_factor(rounded, head_root):
    head_count = head_root.shape[0]
    shaped = rounded.reshape(rounded.shape[0], head_count, HEAD_DIM)
    rightward = jnp.einsum("rhd,hde->rhe", shaped, head_root, preferred_element_type=jnp.float32)
    return rightward.reshape(rounded.shape[0], head_count * HEAD_DIM).astype(jnp.bfloat16)


def shards(
    saved_input,
    query_cotangent,
    key_cotangent,
    query_weight,
    key_weight,
    query_moment,
    key_moment,
    query_row_root,
    key_row_root,
    query_head_root,
    key_head_root,
    query_head_stat,
    key_head_stat,
):
    query_width = query_cotangent.shape[1]
    cotangents = jnp.concatenate([query_cotangent, key_cotangent], axis=1)
    partial_value = sum_by_axis(
        lax.dot_general(
            saved_input, cotangents, (((0,), (0,)), ((), ())), preferred_element_type=jnp.float32
        ),
        FS,
    )
    gradient = of_everyone(partial_value, "rep")
    rounded = gradient.astype(jnp.bfloat16)
    query_rounded = rounded[:, :query_width]
    key_rounded = rounded[:, query_width:]
    query_gram, key_gram = in_one(
        (
            head_gram(query_rounded, query_head_root.shape[0]),
            head_gram(key_rounded, key_head_root.shape[0]),
        ),
        FS,
    )
    query_stat_next = STAT_DECAY * query_head_stat + (1.0 - STAT_DECAY) * query_gram / D
    key_stat_next = STAT_DECAY * key_head_stat + (1.0 - STAT_DECAY) * key_gram / D
    query_right = column_factor(query_rounded, query_head_root)
    key_right = column_factor(key_rounded, key_head_root)
    query_piece, key_piece = side_by_side((query_right, key_right), FS, 0, 1)
    query_pre = jnp.dot(query_row_root, query_piece, preferred_element_type=jnp.float32)
    key_pre = jnp.dot(key_row_root, key_piece, preferred_element_type=jnp.float32)
    query_moment_next = MOMENT_DECAY * query_moment + (1.0 - MOMENT_DECAY) * query_pre
    key_moment_next = MOMENT_DECAY * key_moment + (1.0 - MOMENT_DECAY) * key_pre
    query_wsq, query_msq, key_wsq, key_msq = in_one_2(
        (
            jnp.sum(query_weight * query_weight),
            jnp.sum(query_moment_next * query_moment_next),
            jnp.sum(key_weight * key_weight),
            jnp.sum(key_moment_next * key_moment_next),
        ),
        FS_TP,
    )
    query_step = (
        LEARN_RATE * (jnp.sqrt(query_wsq) / jnp.sqrt(query_msq + EPSILON)) * query_moment_next
    )
    key_step = LEARN_RATE * (jnp.sqrt(key_wsq) / jnp.sqrt(key_msq + EPSILON)) * key_moment_next
    query_next = query_weight - query_step
    key_next = key_weight - key_step
    query_copy, key_copy = side_by_side(
        (query_next.astype(jnp.bfloat16), key_next.astype(jnp.bfloat16)), FS, 0, 1
    )
    return (
        query_step,
        key_step,
        query_next,
        key_next,
        query_copy,
        key_copy,
        query_moment_next,
        key_moment_next,
        query_stat_next,
        key_stat_next,
    )


def solution(mesh):
    split = Mesh(
        mesh.devices.reshape(8, 4, mesh.shape["rep"], mesh.shape["tp"]),
        ("fs_0", "fs_1", "rep", "tp"),
    )
    placed = (
        P(FS_REP, None),
        P(FS_REP, "tp"),
        P(FS_REP, "tp"),
        P(FS, "tp"),
        P(FS, "tp"),
        P(FS, "tp"),
        P(FS, "tp"),
        P(FS, None),
        P(FS, None),
        P("tp", None, None),
        P("tp", None, None),
        P("tp", None, None),
        P("tp", None, None),
    )
    return jax.shard_map(
        shards,
        mesh=split,
        in_specs=placed,
        out_specs=(
            P(FS, "tp"),
            P(FS, "tp"),
            P(FS, "tp"),
            P(FS, "tp"),
            P(None, "tp"),
            P(None, "tp"),
            P(FS, "tp"),
            P(FS, "tp"),
            P("tp", None, None),
            P("tp", None, None),
        ),
        check_vma=False,
    )
```

profile of v0, /device:TPU:2, one launch (start us, length us, event | category | flops | bytes accessed | tf_op | source)
XLA Modules:
  0.0 394.5 jit_solution(3079387826613514579)
XLA Ops:
  7.2 10.7 %convolution_bitcast_fusion = f32[2048,1280]{0,1:T(8,128)} fusion(bf16[1024,2048]{1,0:T(8,128)(2,1)} %param.13, bf16[1024,256]{1,0:T(8,128)(2,1)} %param.15, bf16[1024,1024]{1,0:T(8,128)(2,1)} %param.14), kind=kOutput, calls=%fused_computation | convolution fusion | flops 5373952000 | bytes 17301504 | tf_op jit(solution)/shard_map/dot_general | solution.py:129
  18.0 117.8 %reduce-scatter.5.cloned.1.call-done = f32[256,1280]{0,1:T(8,128)} async-done(((f32[2048,1280]{0,1:T(8,128)}), f32[256,1280]{0,1:T(8,128)}) %reduce-scatter.5.cloned.1.call-update) | async-done | bytes 1310736 | tf_op jit(solution)/shard_map/reduce_scatter | solution.py:22
  135.8 2.8 copy.64
  138.7 24.5 %reduce-scatter.7.cloned.1.call-done = f32[64,1280]{1,0:T(8,128)} async-done(((f32[256,1280]{1,0:T(8,128)}), f32[64,1280]{1,0:T(8,128)}) %reduce-scatter.7.cloned.1.call-update) | async-done | bytes 327696 | tf_op jit(solution)/shard_map/reduce_scatter | solution.py:22
  163.1 1.1 broadcast_in_dim.6
  164.2 21.0 %all_to_all.26 = f32[4,64,1280]{2,1,0:T(8,128)S(1)} all-to-all(f32[4,64,1280]{2,1,0:T(8,128)S(1)} %broadcast_in_dim.6), channel_id=1, replica_groups=mesh['fs_0'=8,'fs_1'=4,'rep'=4,'tp'=2] {'rep'}, dimensions={0} | all-to-all | bytes 2621440 | tf_op jit(solution)/shard_map/all_to_all | solution.py:28
  185.3 0.2 reshape.94
  185.5 0.2 fusion.5
  185.9 0.2 convert_element_type.30
  186.5 0.7 pad_maximum_fusion.1
  187.3 0.6 multiply_reduce_fusion.3
  187.9 0.7 multiply_reduce_fusion.1
  188.6 81.6 %all-gather.3.cloned.1.call-done = bf16[2048,1280]{1,0:T(8,128)(2,1)} async-done(((bf16[64,1280]{1,0:T(8,128)(2,1)}), bf16[2048,1280]{1,0:T(8,128)(2,1)}) %all-gather.3.cloned.1.call-update) | async-done | bytes 5242896 | tf_op jit(solution)/shard_map/all_gather | solution.py:88
  270.2 3.7 multiply_reduce_fusion
  273.9 2.2 multiply_reduce_fusion.2
  276.1 2.7 pad_maximum_fusion.3
  278.8 16.1 %all_to_all.27 = f32[64,1,4]{2,1,0:T(1,128)S(1)} all-to-all(f32[64,1,4]{2,1,0:T(1,128)S(1)} %broadcast_in_dim.7), channel_id=1, replica_groups=mesh['fs_0'=8,'fs_1'=4,'rep'=4,'tp'=2] {'fs_0','fs_1','tp'}, dimensions={0} | all-to-all | bytes 2048 | tf_op jit(solution)/shard_map/all_to_all | solution.py:28
  295.0 0.6 fusion.30
  298.3 0.7 fusion.29
  299.0 0.8 fusion.28
  299.8 0.7 pad_maximum_fusion.2
  300.5 0.3 fusion.20
  301.0 0.2 fusion.24
  301.3 18.1 %all_to_all.28 = f32[32,1,2560]{2,1,0:T(1,128)S(1)} all-to-all(f32[32,1,2560]{2,1,0:T(1,128)S(1)} %bitcast.27), channel_id=1, replica_groups=mesh['fs_0'=8,'fs_1'=4,'rep'=4,'tp'=2] {'fs_0','fs_1'}, dimensions={0} | all-to-all | bytes 655360 | tf_op jit(solution)/shard_map/all_to_all | solution.py:45
  319.4 0.2 reduce_sum.69
  319.8 18.7 %all_to_all.29 = f32[32,1,2560]{2,1,0:T(1,128)S(1)} all-to-all(f32[32,1,2560]{2,1,0:T(1,128)S(1)} %broadcast_in_dim.8), channel_id=1, replica_groups=mesh['fs_0'=8,'fs_1'=4,'rep'=4,'tp'=2] {'fs_0','fs_1'}, dimensions={0} | all-to-all | bytes 655360 | tf_op jit(solution)/shard_map/all_to_all | solution.py:28
  338.5 0.8 reduce.2
  339.5 0.7 fusion.23
  340.1 0.9 fusion.19
  341.0 40.1 %all-gather.5.cloned.1.call-done = bf16[2048,1280]{1,0:T(8,128)(2,1)} async-done(((bf16[64,1280]{1,0:T(8,128)(2,1)}), bf16[2048,1280]{1,0:T(8,128)(2,1)}) %all-gather.5.cloned.1.call-update) | async-done | bytes 5242896 | tf_op jit(solution)/shard_map/all_gather | solution.py:88
  381.1 4.6 %split.18 = bf16[2048,1024]{1,0:T(8,128)(2,1)} slice(bf16[2048,1280]{1,0:T(8,128)(2,1)} %all-gather.5.cloned.1.call-done), slice={[0:2048], [0:1024]} | slice | bytes 8388608 | tf_op jit(solution)/shard_map/split | solution.py:88
  385.7 2.3 split.19
  (47 shorter events, 1.6 us)
Async XLA Ops:
  7.2 263.0 %copy-start = (bf16[64,2048]{1,0:T(8,128)(2,1)S(1)}, bf16[64,2048]{1,0:T(8,128)(2,1)}, u32[]{:S(2)}) copy-start(bf16[64,2048]{1,0:T(8,128)(2,1)} %param.20) | copy-start | bytes 786436
  7.2 128.6 %reduce-scatter.5.cloned.1.call-start = ((), (), s32[]{:S(2)}) async-start(), calls=%async_computation.6 | async-start | bytes 11796480 | tf_op jit(solution)/shard_map/reduce_scatter | solution.py:22
  17.9 145.2 %reduce-scatter.7.cloned.1.call-start = ((), (), s32[]{:S(2)}) async-start(), calls=%async_computation.9 | async-start | bytes 1638400 | tf_op jit(solution)/shard_map/reduce_scatter | solution.py:22
  138.6 46.9 %copy-start.3 = (bf16[16,64,64]{2,1,0:T(8,128)(2,1)S(1)}, bf16[16,64,64]{2,1,0:T(8,128)(2,1)}, u32[]{:S(2)}) copy-start(bf16[16,64,64]{2,1,0:T(8,128)(2,1)} %param.22) | copy-start | bytes 393220
  138.6 47.6 %copy-start.7 = (bf16[4,64,64]{2,1,0:T(8,128)(2,1)S(1)}, bf16[4,64,64]{2,1,0:T(8,128)(2,1)}, u32[]{:S(2)}) copy-start(bf16[4,64,64]{2,1,0:T(8,128)(2,1)} %param.23) | copy-start | bytes 98308
  138.6 48.7 %copy-start.4 = (f32[64,256]{1,0:T(8,128)S(1)}, f32[64,256]{1,0:T(8,128)}, u32[]{:S(2)}) copy-start(f32[64,256]{1,0:T(8,128)} %param.17) | copy-start | bytes 196612
  138.6 131.6 %all-gather.3.cloned.1.call-start = ((), (), s32[]{:S(2)}) async-start(), calls=%async_computation.7 | async-start | bytes 5406720 | tf_op jit(solution)/shard_map/all_gather | solution.py:88
  164.2 23.7 %copy-start.1 = (f32[64,1024]{1,0:T(8,128)S(1)}, f32[64,1024]{1,0:T(8,128)}, u32[]{:S(2)}) copy-start(f32[64,1024]{1,0:T(8,128)} %param.16) | copy-start | bytes 786436
  164.2 106.0 %copy-start.9 = (f32[64,1024]{1,0:T(8,128)S(1)}, f32[64,1024]{1,0:T(8,128)}, u32[]{:S(2)}) copy-start(f32[64,1024]{1,0:T(8,128)} %param.18) | copy-start | bytes 786436
  185.5 88.4 %copy-start.10 = (bf16[64,2048]{1,0:T(8,128)(2,1)S(1)}, bf16[64,2048]{1,0:T(8,128)(2,1)}, u32[]{:S(2)}) copy-start(bf16[64,2048]{1,0:T(8,128)(2,1)} %param.21) | copy-start | bytes 786436
  185.5 88.4 %copy-start.11 = (f32[64,256]{1,0:T(8,128)S(1)}, f32[64,256]{1,0:T(8,128)}, u32[]{:S(2)}) copy-start(f32[64,256]{1,0:T(8,128)} %param.19) | copy-start | bytes 196612
  187.2 193.8 %all-gather.5.cloned.1.call-start = ((), (), s32[]{:S(2)}) async-start(), calls=%async_computation.8 | async-start | bytes 5406720 | tf_op jit(solution)/shard_map/all_gather | solution.py:88
  273.9 65.4 %copy-start.5 = (f32[64,1024]{1,0:T(8,128)}, f32[64,1024]{1,0:T(8,128)S(1)}, u32[]{:S(2)}) copy-start(f32[64,1024]{1,0:T(8,128)S(1)} %get-tuple-element.23) | copy-start | bytes 786436
  276.1 63.3 %copy-start.8 = (f32[64,256]{1,0:T(8,128)}, f32[64,256]{1,0:T(8,128)S(1)}, u32[]{:S(2)}) copy-start(f32[64,256]{1,0:T(8,128)S(1)} %get-tuple-element.21) | copy-start | bytes 196612
  278.8 60.7 %copy-start.6 = (f32[4,64,64]{2,1,0:T(8,128)S(1)}, f32[4,64,64]{2,1,0:T(8,128)}, u32[]{:S(2)}) copy-start(f32[4,64,64]{2,1,0:T(8,128)} %param.25) | copy-start | bytes 196612
  299.0 41.1 %copy-start.2 = (f32[16,64,64]{2,1,0:T(8,128)S(1)}, f32[16,64,64]{2,1,0:T(8,128)}, u32[]{:S(2)}) copy-start(f32[16,64,64]{2,1,0:T(8,128)} %param.24) | copy-start | bytes 786436
Sparse Core Ops, SparseCore 0:
  18.1 117.6 reduce-scatter.4
  138.9 24.1 reduce-scatter.6
  187.4 82.7 all-gather.2
  300.7 80.3 all-gather.4
where the time goes:
time: 396 us; the launch traced here: 394 us
  waiting for transfers between devices  264 us (67%)
  blocking collectives  73.9 us (19%)
  matrix products  17.4 us (4%)
  between operations  16.8 us (4%)
  local copies, waits for them, and re-layouts  12.8 us (3%)
  other arithmetic  9.48 us (2%)
    reduce_scatter x2, waiting for transfers between devices, sum_by_axis(): total = lax.psum_scatter(total, axis, scatter_dimension=0, tiled=True)  142 us
    all_gather x2, waiting for transfers between devices, side_by_side(): lax.all_gather(both, axis, axis=dim, tiled=True)  122 us
    all_to_all x3, blocking collectives, copy_for_each(): lax.all_to_all(jnp.broadcast_to(value[None], (count, *value.shape)), axis...  55.8 us
    all_to_all x1, blocking collectives, sum_at_owner(): lax.all_to_all(parts, axis, split_axis=0, concat_axis=0, tiled=True)  18.1 us
    dot_general x1, matrix products, shards(): lax.dot_general(saved_input, cotangents, (((0,), (0,)), ((), ())), prefer...  10.7 us
  transfers between devices with their start and end apart: 4, of which 4 were waited for; matrix products, arithmetic and copies ran while one was open for 1% of the time, Pallas kernels for 0%

commit v1 on v0

v1 whole, which is shorter than its diff:
```python
import functools

import jax
import jax.numpy as jnp
from jax import lax
from jax.experimental import pallas as pl
from jax.experimental.pallas import tpu as pltpu
from jax.sharding import Mesh
from jax.sharding import PartitionSpec as P

D = 2048
HEAD_DIM = 64
NZ, NX, NY = 8, 4, 4
Z, X, Y = "fs_0", "fs_1", "rep"
FS = (Z, X)
FS_TP = (Z, X, "tp")
FS_REP = (Z, X, Y)
ROWS = (Y, X, Z)
MOMENT_DECAY = 0.8
STAT_DECAY = 0.5
LEARN_RATE = 0.1
EPSILON = 1e-06
MESH = pl.DeviceIdType.MESH
WA, WB, WC = 512, 384, 384
BLK = 16


def plane_pairs():
    return [(dy, dx) for dy in range(NY) for dx in range(NX) if dy or dx]


def greet(peers):
    barrier = pltpu.get_barrier_semaphore()
    for dev in peers:
        pl.semaphore_signal(barrier, inc=1, device_id=dev, device_id_type=MESH)
    pl.semaphore_wait(barrier, len(peers))


def ring_slots(n):
    slots = [(n // 2, 0, None)]
    for k in range(1, n // 2):
        slots.append((n // 2 - k, 1, 2 * k - 3 if k >= 2 else None))
        slots.append((n // 2 - k, 0, 2 * k - 2))
    return slots


class Ring:
    def __init__(self, axis, n, region, recv, send_sem, recv_sem, add):
        self.n, self.me = n, lax.axis_index(axis)
        self.region, self.recv, self.add = region, recv, add
        self.slots = ring_slots(n)
        self.copies = {}
        for way in range(2):
            to = lax.rem(self.me + (1 if way == 0 else n - 1), n)
            for j, (dist, half, _) in enumerate(self.slots):
                self.copies[way, j] = pltpu.make_async_remote_copy(
                    src_ref=region(self.chunk(way, dist), half ^ way),
                    dst_ref=recv.at[way, j],
                    send_sem=send_sem.at[way, j],
                    recv_sem=recv_sem.at[way, j],
                    device_id={axis: to},
                    device_id_type=MESH,
                )

    def chunk(self, way, dist):
        return lax.rem(self.me + (dist if way == 0 else self.n - dist), self.n)

    def send(self, j):
        for way in range(2):
            dist, half, source = self.slots[j]
            if source is not None:
                self.copies[way, source].wait_recv()
                self.add(self.chunk(way, dist), half ^ way, self.recv.at[way, source])
            self.copies[way, j].start()

    def finish(self):
        for j in (self.n - 3, self.n - 2):
            for way in range(2):
                self.copies[way, j].wait_recv()
                self.add(self.me, self.slots[j][1] ^ way, self.recv.at[way, j])

    def drain(self):
        for copy in self.copies.values():
            copy.wait_send()


def gradient_kernel(
    x_ref, qc_ref, kc_ref, out_ref,
    ga, gb, gc, ra, rb, rc, pa, b1, c1, b2, c2,
    a_ss, a_rs, b_ss, b_rs, c_ss, c_rs, pa_ss, pa_rs, b1_ss, b1_rs, c1_ss, c1_rs, b2_ss, b2_rs, c2_ss, c2_rs,
):
    z, x, y = lax.axis_index(Z), lax.axis_index(X), lax.axis_index(Y)
    z_of = [lax.rem(z + d, NZ) for d in range(NZ)]
    x_of = [lax.rem(x + d, NX) for d in range(NX)]
    y_of = [lax.rem(y + d, NY) for d in range(NY)]
    greet(
        [{Z: z_of[d]} for d in range(1, NZ)]
        + [{Y: y_of[dy], X: x_of[dx]} for dy, dx in plane_pairs()]
    )

    def product(start, count, cot, low, width):
        return lax.dot_general(
            x_ref[:, pl.ds(pl.multiple_of(start, 128), count)],
            cot[:, low : low + width],
            (((0,), (0,)), ((), ())),
            preferred_element_type=jnp.float32,
        )

    def add_a(chunk, half, recv):
        for y2 in range(2):
            def body(x2, _):
                at = (2 * half + y2, x2, chunk)
                ga[at] = ga[at] + recv[y2, x2]
                return 0
            lax.fori_loop(0, NX, body, 0)

    def add_b(chunk, half, recv):
        for y2 in range(2):
            def body(z2, _):
                at = (2 * half + y2, chunk, z2)
                gb[at] = gb[at] + recv[y2, z2]
                return 0
            lax.fori_loop(0, NZ, body, 0)

    def add_c(chunk, half, recv):
        for x2 in range(2):
            def body(z2, _):
                at = (chunk, 2 * half + x2, z2)
                gc[at] = gc[at] + recv[x2, z2]
                return 0
            lax.fori_loop(0, NZ, body, 0)

    ring_a = Ring(Z, NZ, lambda c, h: ga.at[pl.ds(2 * h, 2), :, c], ra, a_ss, a_rs, add_a)
    ring_b = Ring(X, NX, lambda c, h: gb.at[pl.ds(2 * h, 2), c], rb, b_ss, b_rs, add_b)
    ring_c = Ring(Y, NY, lambda c, h: gc.at[c, pl.ds(2 * h, 2)], rc, c_ss, c_rs, add_c)

    def make_a(yy, _):
        ga[yy] = product(yy * 512, 512, qc_ref, 0, WA).reshape(NX, NZ, BLK, WA)
        return 0

    def make_b(chunk):
        def body(yy, _):
            gb[yy, chunk] = product(yy * 512 + chunk * 128, 128, qc_ref, WA, WB).reshape(NZ, BLK, WB)
            return 0
        lax.fori_loop(0, NY, body, 0)

    def make_c(chunk):
        gc[chunk, :, :, :, 0:128] = product(chunk * 512, 512, qc_ref, WA + WB, 128).reshape(NX, NZ, BLK, 128)
        gc[chunk, :, :, :, 128:WC] = product(chunk * 512, 512, kc_ref, 0, 256).reshape(NX, NZ, BLK, 256)

    lax.fori_loop(0, NY, make_a, 0)
    ring_a.send(0)
    ring_a.send(1)
    make_b(x_of[2])
    ring_b.send(0)
    make_c(y_of[2])
    ring_c.send(0)
    make_b(x_of[1])
    make_b(x_of[3])
    ring_b.send(1)
    make_c(y_of[1])
    make_c(y_of[3])
    ring_c.send(1)
    ring_a.send(2)
    make_b(x_of[0])
    make_c(y_of[0])
    ring_a.send(3)
    ring_b.send(2)
    ring_c.send(2)
    ring_a.send(4)
    ring_a.send(5)
    ring_a.send(6)

    def direct(src, dst, ss, rs, d, dev):
        return pltpu.make_async_remote_copy(
            src_ref=src, dst_ref=dst.at[d], send_sem=ss.at[d], recv_sem=rs.at[d],
            device_id=dev, device_id_type=MESH,
        )

    ring_c.finish()
    to_c1 = [direct(gc.at[y, x_of[d]], c1, c1_ss, c1_rs, d - 1, {X: x_of[d]}) for d in (1, 3, 2)]
    for copy in to_c1:
        copy.start()
    ring_b.finish()
    to_b1 = [direct(gb.at[y_of[d], x], b1, b1_ss, b1_rs, d - 1, {Y: y_of[d]}) for d in (1, 3, 2)]
    for copy in to_b1:
        copy.start()

    for copy in to_c1:
        copy.wait_recv()
    def sum_c(zz, _):
        gc[y, x, zz] = (gc[y, x, zz] + c1[0, zz]) + (c1[1, zz] + c1[2, zz])
        return 0
    lax.fori_loop(0, NZ, sum_c, 0)
    to_c2 = [direct(gc.at[y, x, z_of[d]], c2, c2_ss, c2_rs, d - 1, {Z: z_of[d]}) for d in range(1, NZ)]
    for copy in to_c2:
        copy.start()

    ring_a.finish()
    to_pa = [
        direct(ga.at[y_of[dy], x_of[dx], z], pa, pa_ss, pa_rs, i, {Y: y_of[dy], X: x_of[dx]})
        for i, (dy, dx) in enumerate(plane_pairs())
    ]
    for copy in to_pa:
        copy.start()

    for copy in to_b1:
        copy.wait_recv()
    def sum_b(zz, _):
        gb[y, x, zz] = (gb[y, x, zz] + b1[0, zz]) + (b1[1, zz] + b1[2, zz])
        return 0
    lax.fori_loop(0, NZ, sum_b, 0)
    to_b2 = [direct(gb.at[y, x, z_of[d]], b2, b2_ss, b2_rs, d - 1, {Z: z_of[d]}) for d in range(1, NZ)]
    for copy in to_b2:
        copy.start()

    for copy in to_c2:
        copy.wait_recv()
    total = gc[y, x, z]
    for d in range(NZ - 1):
        total = total + c2[d]
    out_ref[:, WA + WB :] = total
    for copy in to_pa:
        copy.wait_recv()
    total = ga[y, x, z]
    for d in range(NX * NY - 1):
        total = total + pa[d]
    out_ref[:, :WA] = total
    for copy in to_b2:
        copy.wait_recv()
    total = gb[y, x, z]
    for d in range(NZ - 1):
        total = total + b2[d]
    out_ref[:, WA : WA + WB] = total

    for ring in (ring_a, ring_b, ring_c):
        ring.drain()
    for copy in to_c1 + to_b1 + to_c2 + to_pa + to_b2:
        copy.wait_send()


def gradient_block(x, qc, kc):
    f32, dma = jnp.float32, pltpu.SemaphoreType.DMA
    vm = pltpu.VMEM
    space = pl.BlockSpec(memory_space=pltpu.VMEM)
    sems = []
    for shape in ((2, 7), (2, 3), (2, 3), (15,), (3,), (3,), (7,), (7,)):
        sems += [dma(shape), dma(shape)]
    return pl.pallas_call(
        gradient_kernel,
        out_shape=jax.ShapeDtypeStruct((BLK, WA + WB + WC), f32),
        in_specs=[space] * 3,
        out_specs=space,
        scratch_shapes=[
            vm((NY, NX, NZ, BLK, WA), f32),
            vm((NY, NX, NZ, BLK, WB), f32),
            vm((NY, NX, NZ, BLK, WC), f32),
            vm((2, 7, 2, NX, BLK, WA), f32),
            vm((2, 3, 2, NZ, BLK, WB), f32),
            vm((2, 3, 2, NZ, BLK, WC), f32),
            vm((15, BLK, WA), f32),
            vm((3, NZ, BLK, WB), f32),
            vm((3, NZ, BLK, WC), f32),
            vm((7, BLK, WB), f32),
            vm((7, BLK, WC), f32),
        ] + sems,
        compiler_params=pltpu.CompilerParams(
            collective_id=0, has_side_effects=True, vmem_limit_bytes=60 * 2**20
        ),
        name="gradient_sum",
    )(x, qc, kc)


def head_gram(rounded, head_count):
    shaped = rounded.reshape(rounded.shape[0], head_count, HEAD_DIM)
    return jnp.einsum("rhd,rhe->hde", shaped, shaped, preferred_element_type=jnp.float32)


def column_factor(rounded, head_root):
    head_count = head_root.shape[0]
    shaped = rounded.reshape(rounded.shape[0], head_count, HEAD_DIM)
    rightward = jnp.einsum("rhd,hde->rhe", shaped, head_root, preferred_element_type=jnp.float32)
    return rightward.reshape(rounded.shape[0], head_count * HEAD_DIM).astype(jnp.bfloat16)


def shards(x, qc, kc, qw, kw, qm, km, ql, kl, qr, kr, qs, ks):
    qn = qc.shape[1]
    grad = gradient_block(x, qc, kc)
    rounded = grad.astype(jnp.bfloat16)
    root = jnp.concatenate([qr, kr], axis=0)
    right = column_factor(rounded, root)
    piece = lax.all_gather(right, ROWS, axis=0, tiled=True)
    gram = lax.psum(head_gram(rounded, root.shape[0]), ROWS)
    hq = qr.shape[0]
    qs2 = STAT_DECAY * qs + (1.0 - STAT_DECAY) * gram[:hq] / D
    ks2 = STAT_DECAY * ks + (1.0 - STAT_DECAY) * gram[hq:] / D
    qp = jnp.dot(ql, piece[:, :qn], preferred_element_type=jnp.float32)
    kp = jnp.dot(kl, piece[:, qn:], preferred_element_type=jnp.float32)
    qm2 = MOMENT_DECAY * qm + (1.0 - MOMENT_DECAY) * qp
    km2 = MOMENT_DECAY * km + (1.0 - MOMENT_DECAY) * kp
    sums = jnp.stack([jnp.sum(qw * qw), jnp.sum(qm2 * qm2), jnp.sum(kw * kw), jnp.sum(km2 * km2)])
    n = lax.axis_size(FS_TP)
    every = lax.all_to_all(jnp.broadcast_to(sums[None], (n, 4)), FS_TP, 0, 0, tiled=True).sum(axis=0)
    qstep = LEARN_RATE * (jnp.sqrt(every[0]) / jnp.sqrt(every[1] + EPSILON)) * qm2
    kstep = LEARN_RATE * (jnp.sqrt(every[2]) / jnp.sqrt(every[3] + EPSILON)) * km2
    qn2 = qw - qstep
    kn2 = kw - kstep
    both = jnp.concatenate([qn2, kn2], axis=1).astype(jnp.bfloat16)
    mine = lax.dynamic_slice_in_dim(both, lax.axis_index(Y) * BLK, BLK, 0)
    copy = lax.all_gather(mine, FS_REP, axis=0, tiled=True)
    return qstep, kstep, qn2, kn2, copy[:, :qn], copy[:, qn:], qm2, km2, qs2, ks2


def solution(mesh):
    split = Mesh(
        mesh.devices.reshape(NZ, NX, NY, mesh.shape["tp"]), (Z, X, Y, "tp")
    )
    row = P(FS, "tp")
    head = P("tp", None, None)
    whole = P(None, "tp")
    tok = P(FS_REP, "tp")
    return jax.shard_map(
        shards, mesh=split,
        in_specs=(P(FS_REP, None), tok, tok, row, row, row, row, P(FS, None), P(FS, None), head, head, head, head),
        out_specs=(row, row, row, row, whole, whole, row, row, head, head),
        check_vma=False,
    )
```

time: 396 us -> 569 us (1.44)
  waiting for transfers between devices: 264 us -> 450 us
  blocking collectives: 73.9 us -> 0 us
  Pallas kernels: 0 us -> 67.2 us
  matrix products: 17.4 us -> 7.21 us
  starting transfers between devices: 0.16 us -> 7.7 us
    psum x0 -> x1, waiting for transfers between devices: none -> 213 us  [shards(): gram = lax.psum(head_gram(rounded, root.shape[0]), ROWS)]
    reduce_scatter x2 -> x0, waiting for transfers between devices: 142 us -> none  [sum_by_axis(): total = lax.psum_scatter(total, axis, scatter_dimension=0, tiled=True)]
    all_gather x2, waiting for transfers between devices: 122 us -> 230 us  [the longest x1 116 us: shards(): copy = lax.all_gather(mine, FS_REP, axis=0, tiled=True)]
    all_to_all x4 -> x0, blocking collectives: 73.9 us -> none  [the longest x3 55.8 us: copy_for_each(): lax.all_to_all(jnp.broadcast_to(value[None], (count, *value.shape)), axis...]
    pallas_call x0 -> x1, Pallas kernels: none -> 67.2 us  [gradient_block(): pl.pallas_call(gradient_kernel, out_shape=jax.ShapeDtypeStruct((BLK, WA +...]
    dot_general x3 -> x2, matrix products: 16.6 us -> 5.9 us  [the longest x1 3.67 us: shards(): qp = jnp.dot(ql, piece[:, :qn], preferred_element_type=jnp.float32)]
    all_to_all x0 -> x1, starting transfers between devices: none -> 7.58 us  [shards(): lax.all_to_all(jnp.broadcast_to(sums[None], (n, 4)), FS_TP, 0, 0, tiled=T...]
    all_to_all x0 -> x1, waiting for transfers between devices: none -> 7.3 us  [shards(): lax.all_to_all(jnp.broadcast_to(sums[None], (n, 4)), FS_TP, 0, 0, tiled=T...]
  transfers between devices with their start and end apart: 4 -> 4, of which waited for: 4 -> 4; matrix products, arithmetic and copies ran while one was open for 1% -> 2% of each run, Pallas kernels for 0% -> 0%
where the time goes in v1:
time: 569 us
  waiting for transfers between devices  450 us (79%)
  Pallas kernels  67.2 us (12%)
  between operations  16.7 us (3%)
  other arithmetic  10.5 us (2%)
  local copies, waits for them, and re-layouts  9.09 us (2%)
  starting transfers between devices  7.7 us (1%)
  matrix products  7.21 us (1%)
    psum x1, waiting for transfers between devices, shards(): gram = lax.psum(head_gram(rounded, root.shape[0]), ROWS)  213 us
    all_gather x1, waiting for transfers between devices, shards(): copy = lax.all_gather(mine, FS_REP, axis=0, tiled=True)  116 us
    all_gather x1, waiting for transfers between devices, shards(): piece = lax.all_gather(right, ROWS, axis=0, tiled=True)  114 us
    pallas_call x1, Pallas kernels, gradient_block(): pl.pallas_call(gradient_kernel, out_shape=jax.ShapeDtypeStruct((BLK, WA +...  67.2 us
  transfers between devices with their start and end apart: 4, of which 4 were waited for; matrix products, arithmetic and copies ran while one was open for 2% of the time, Pallas kernels for 0%

profile of v1, /device:TPU:2, one launch (start us, length us, event | category | flops | bytes accessed | tf_op | source)
XLA Modules:
  0.0 568.7 jit_solution(4188922881654490155)
XLA Ops:
  7.3 0.0 all-gather.3.cloned.1.call-start
  7.3 67.2 %gradient_sum.1 = f32[16,1280]{1,0:T(8,128)} custom-call(bf16[1024,2048]{1,0:T(8,128)(2,1)} %x_ref.1, bf16[1024,1024]{1,0:T(8,128)(2,1)} %qc_ref.1, bf16[1024,256]{1,0:T(8,128)(2,1)} %kc_ref.1), custom_call_target="tpu_custom_call" | custom-call | tf_op jit(solution)/shard_map/gradient_sum/pallas_call | solution.py:249
  74.6 0.9 convert_element_type.13
  75.5 0.1 reshape.46
  75.6 0.2 fusion.11
  75.8 0.7 convert_element_type.16
  76.6 0.0 all-gather.3.cloned.1.call-update
  76.6 0.6 multiply_reduce_fusion.3
  77.2 0.7 multiply_reduce_fusion.1
  77.9 113.8 %all-gather.3.cloned.1.call-done = bf16[2048,1280]{1,0:T(8,128)(2,1)} async-done(((bf16[16,1280]{1,0:T(8,128)(2,1)}), bf16[2048,1280]{1,0:T(8,128)(2,1)}) %all-gather.3.cloned.1.call-update) | async-done | bytes 5242896 | tf_op jit(solution)/shard_map/all_gather | solution.py:292
  191.7 3.7 multiply_reduce_fusion
  195.4 2.2 multiply_reduce_fusion.2
  197.6 2.7 pad_maximum_fusion
  200.3 0.6 broadcast_in_dim.2
  200.9 7.6 %all-to-all-start = ((f32[64,1,4]{2,1,0:T(1,128)}), f32[64,1,4]{2,1,0:T(1,128)S(1)}, u32[]{:S(2)}, u32[]{:S(2)}) async-start(f32[64,1,4]{2,1,0:T(1,128)} %broadcast_in_dim.2), calls=%async_computation | async-start | bytes 65536 | tf_op jit(solution)/shard_map/all_to_all | solution.py:303
  208.5 0.0 all-reduce.2.cloned.1.call-start
  208.5 1.1 fusion.20
  209.7 0.0 all-reduce.2.cloned.1.call-update
  209.7 0.0 all-gather.5.cloned.1.call-start
  209.7 7.3 %all-to-all-done = f32[64,1,4]{2,1,0:T(1,128)S(1)} async-done(((f32[64,1,4]{2,1,0:T(1,128)}), f32[64,1,4]{2,1,0:T(1,128)S(1)}, u32[]{:S(2)}, u32[]{:S(2)}) %all-to-all-start) | async-done | bytes 1056 | tf_op jit(solution)/shard_map/all_to_all | solution.py:303
  217.0 0.1 reduce_sum.49
  217.1 0.6 fusion.27
  220.5 0.8 fusion.26
  221.3 0.7 fusion.25
  222.0 0.6 fusion.23
  222.6 0.0 all-gather.5.cloned.1.call-update
  222.6 213.1 %all-reduce.2.cloned.1.call-done = f32[20,64,64]{2,1,0:T(8,128)} async-done(((f32[20,64,64]{2,1,0:T(8,128)}), f32[20,64,64]{2,1,0:T(8,128)}) %all-reduce.2.cloned.1.call-update) | async-done | bytes 327696 | tf_op jit(solution)/shard_map/psum | solution.py:293
  435.7 1.6 fusion.19
  437.3 1.9 fusion.15
  439.2 116.1 %all-gather.5.cloned.1.call-done = bf16[2048,1280]{1,0:T(8,128)(2,1)} async-done(((bf16[16,1280]{1,0:T(8,128)(2,1)}), bf16[2048,1280]{1,0:T(8,128)(2,1)}) %all-gather.5.cloned.1.call-update) | async-done | bytes 5242896 | tf_op jit(solution)/shard_map/all_gather | solution.py:310
  555.3 4.6 slice.42
  559.9 2.3 slice.43
  (25 shorter events, 0.1 us)
Async XLA Ops:
  7.2 184.5 %copy-start = (bf16[64,2048]{1,0:T(8,128)(2,1)S(1)}, bf16[64,2048]{1,0:T(8,128)(2,1)}, u32[]{:S(2)}) copy-start(bf16[64,2048]{1,0:T(8,128)(2,1)} %param.20) | copy-start | bytes 786436
  7.2 68.4 %copy-start.10 = (bf16[4,64,64]{2,1,0:T(8,128)(2,1)S(1)}, bf16[4,64,64]{2,1,0:T(8,128)(2,1)}, u32[]{:S(2)}) copy-start(bf16[4,64,64]{2,1,0:T(8,128)(2,1)} %param.23) | copy-start | bytes 98308
  7.2 68.4 %copy-start.7 = (bf16[16,64,64]{2,1,0:T(8,128)(2,1)S(1)}, bf16[16,64,64]{2,1,0:T(8,128)(2,1)}, u32[]{:S(2)}) copy-start(bf16[16,64,64]{2,1,0:T(8,128)(2,1)} %param.22) | copy-start | bytes 393220
  7.2 69.4 %copy-start.3 = (f32[64,256]{1,0:T(8,128)S(1)}, f32[64,256]{1,0:T(8,128)}, u32[]{:S(2)}) copy-start(f32[64,256]{1,0:T(8,128)} %param.17) | copy-start | bytes 196612
  7.2 70.0 %copy-start.1 = (f32[64,1024]{1,0:T(8,128)S(1)}, f32[64,1024]{1,0:T(8,128)}, u32[]{:S(2)}) copy-start(f32[64,1024]{1,0:T(8,128)} %param.16) | copy-start | bytes 786436
  7.2 184.5 %copy-start.8 = (f32[64,1024]{1,0:T(8,128)S(1)}, f32[64,1024]{1,0:T(8,128)}, u32[]{:S(2)}) copy-start(f32[64,1024]{1,0:T(8,128)} %param.18) | copy-start | bytes 786436
  7.2 188.1 %copy-start.9 = (bf16[64,2048]{1,0:T(8,128)(2,1)S(1)}, bf16[64,2048]{1,0:T(8,128)(2,1)}, u32[]{:S(2)}) copy-start(bf16[64,2048]{1,0:T(8,128)(2,1)} %param.21) | copy-start | bytes 786436
  7.3 188.1 %copy-start.11 = (f32[64,256]{1,0:T(8,128)S(1)}, f32[64,256]{1,0:T(8,128)}, u32[]{:S(2)}) copy-start(f32[64,256]{1,0:T(8,128)} %param.19) | copy-start | bytes 196612
  7.3 184.4 %all-gather.3.cloned.1.call-start = ((), (), s32[]{:S(2)}) async-start(), calls=%async_computation.1 | async-start | bytes 5283840 | tf_op jit(solution)/shard_map/all_gather | solution.py:292
  77.2 358.5 %copy-start.5 = (f32[4,64,64]{2,1,0:T(8,128)S(1)}, f32[4,64,64]{2,1,0:T(8,128)}, u32[]{:S(2)}) copy-start(f32[4,64,64]{2,1,0:T(8,128)} %param.25) | copy-start | bytes 196612
  77.9 359.4 %copy-start.2 = (f32[16,64,64]{2,1,0:T(8,128)S(1)}, f32[16,64,64]{2,1,0:T(8,128)}, u32[]{:S(2)}) copy-start(f32[16,64,64]{2,1,0:T(8,128)} %param.24) | copy-start | bytes 786436
  195.4 364.5 %copy-start.4 = (f32[64,1024]{1,0:T(8,128)}, f32[64,1024]{1,0:T(8,128)S(1)}, u32[]{:S(2)}) copy-start(f32[64,1024]{1,0:T(8,128)S(1)} %get-tuple-element.23) | copy-start | bytes 786436
  197.6 362.3 %copy-start.6 = (f32[64,256]{1,0:T(8,128)}, f32[64,256]{1,0:T(8,128)S(1)}, u32[]{:S(2)}) copy-start(f32[64,256]{1,0:T(8,128)S(1)} %get-tuple-element.21) | copy-start | bytes 196612
  200.9 16.1 %all-to-all-start = ((f32[64,1,4]{2,1,0:T(1,128)}), f32[64,1,4]{2,1,0:T(1,128)S(1)}, u32[]{:S(2)}, u32[]{:S(2)}) async-start(f32[64,1,4]{2,1,0:T(1,128)} %broadcast_in_dim.2), calls=%async_computation | async-start | bytes 65536 | tf_op jit(solution)/shard_map/all_to_all | solution.py:303
  208.5 227.2 %all-reduce.2.cloned.1.call-start = ((), (), s32[]{:S(2)}) async-start(), calls=%async_computation.3 | async-start | bytes 1310720 | tf_op jit(solution)/shard_map/psum | solution.py:293
  209.7 345.6 %all-gather.5.cloned.1.call-start = ((), (), s32[]{:S(2)}) async-start(), calls=%async_computation.2 | async-start | bytes 5283840 | tf_op jit(solution)/shard_map/all_gather | solution.py:310
Sparse Core Ops, SparseCore 0:
  76.7 114.9 all-gather.2
  215.2 220.4 all-reduce.1
  439.8 115.4 all-gather.4

commit v2 on v1

v2 whole, which is shorter than its diff:
```python
import jax
import jax.numpy as jnp
from jax import lax
from jax.experimental import pallas as pl
from jax.experimental.pallas import tpu as pltpu
from jax.sharding import Mesh
from jax.sharding import PartitionSpec as P

D = 2048
HEAD_DIM = 64
NZ, NX, NY, NT = 8, 4, 4, 2
Z, X, Y, T = "fs_0", "fs_1", "rep", "tp"
FS = (Z, X)
FS_REP = (Z, X, Y)
MOMENT_DECAY = 0.8
STAT_DECAY = 0.5
LEARN_RATE = 0.1
EPSILON = 1e-06
MESH = pl.DeviceIdType.MESH
QN, KN = 1024, 256
WA, WB, WC = 512, 384, 384
WP = 640
BLK = 16
PAIRS = 10
QPAIRS = 8
COPIES = 256
F32, BF16 = jnp.float32, jnp.bfloat16


class Net:
    def __init__(self, send_sem, recv_sem):
        self.send_sem, self.recv_sem, self.used, self.sent = send_sem, recv_sem, 0, []

    def copy(self, src, dst, dev, landing=None):
        k = self.used
        self.used += 1
        copies = [
            pltpu.make_async_remote_copy(
                src_ref=a, dst_ref=b, send_sem=self.send_sem.at[k], recv_sem=self.recv_sem.at[k],
                device_id=dev, device_id_type=MESH,
            )
            for a, b in ((src, dst), (dst, dst) if landing is None else (landing, landing))
        ]
        return Copy(self, *copies)

    def drain(self):
        for copy in self.sent:
            copy.wait_send()


class Copy:
    def __init__(self, net, out, into):
        self.net, self.out, self.into = net, out, into

    def start(self):
        self.out.start()
        self.net.sent.append(self.out)

    def wait(self):
        self.into.wait_recv()


def start_all(copies):
    for copy in copies:
        copy.start()


def wait_all(copies):
    for copy in copies:
        copy.wait()


class Ring:
    def __init__(self, axis, n):
        self.n, self.me = n, lax.axis_index(axis)
        self.copies = {}
        self.device = [{axis: self.place(way, 1)} for way in range(2)]

    def place(self, way, dist):
        return lax.rem(self.me + (dist if way == 0 else self.n - dist), self.n)


class RingSum(Ring):
    def __init__(self, net, axis, n, region, recv, add):
        super().__init__(axis, n)
        self.recv, self.add = recv, add
        self.slots = [(n // 2, 0, None)]
        for k in range(1, n // 2):
            self.slots.append((n // 2 - k, 1, 2 * k - 3 if k >= 2 else None))
            self.slots.append((n // 2 - k, 0, 2 * k - 2))
        for way in range(2):
            for j, (dist, half, _) in enumerate(self.slots):
                self.copies[way, j] = net.copy(
                    region(self.place(way, dist), half ^ way), recv.at[way, j], self.device[way]
                )

    def send(self, j):
        for way in range(2):
            dist, half, source = self.slots[j]
            if source is not None:
                self.copies[way, source].wait()
                self.add(self.place(way, dist), half ^ way, self.recv.at[way, source])
            self.copies[way, j].start()

    def finish(self):
        for j in (self.n - 3, self.n - 2):
            for way in range(2):
                self.copies[way, j].wait()
                self.add(self.me, self.slots[j][1] ^ way, self.recv.at[way, j])


class RingGather(Ring):
    def __init__(self, net, axis, n, regions):
        super().__init__(axis, n)
        slots = [(j // 2, j % 2) for j in range(n - 1)]
        for way in range(2):
            for j, (k, half) in enumerate(slots):
                held = regions(self.place(1 - way, k), half ^ way)
                coming = regions(self.place(1 - way, k + 1), half ^ way)
                self.copies[way, j] = [
                    net.copy(a, a, self.device[way], b) for a, b in zip(held, coming)
                ]

    def send(self, j):
        for way in range(2):
            if j >= 2:
                wait_all(self.copies[way, j - 2])
            start_all(self.copies[way, j])

    def finish(self):
        for j in (self.n - 3, self.n - 2):
            for way in range(2):
                wait_all(self.copies[way, j])


def lane_sums(value):
    total = value[:, 0:128]
    for i in range(1, value.shape[1] // 128):
        total = total + value[:, 128 * i : 128 * (i + 1)]
    return jnp.sum(total, axis=0, keepdims=True)


def step_kernel(
    x_ref, qc_ref, kc_ref, qw_ref, kw_ref, qm_ref, km_ref, ql_ref, kl_ref, qr_ref, kr_ref, qs_ref, ks_ref,
    qstep_ref, kstep_ref, qnext_ref, knext_ref, qcopy_ref, kcopy_ref, qm2_ref, km2_ref, qs2_ref, ks2_ref,
    ga, gb, gc, ra, rb, rc, pa, b1, c1, b2, c2,
    gath, roots, pp, pr, mbuf, gp, gr, gfin, plane, zed, send_sem, recv_sem,
):
    z, x, y, t = (lax.axis_index(a) for a in (Z, X, Y, T))
    z_of = [lax.rem(z + d, NZ) for d in range(NZ)]
    x_of = [lax.rem(x + d, NX) for d in range(NX)]
    y_of = [lax.rem(y + d, NY) for d in range(NY)]
    spots = [(dy, dx) for dy in range(NY) for dx in range(NX)]
    others = [(dy, dx, dt) for dy, dx in spots for dt in range(NT) if dy or dx or dt]
    net = Net(send_sem, recv_sem)

    peers = [{Z: z_of[d]} for d in range(1, NZ)] + [
        {Y: y_of[dy], X: x_of[dx], T: lax.rem(t + dt, NT)} for dy, dx, dt in others
    ]
    barrier = pltpu.get_barrier_semaphore()
    for dev in peers:
        pl.semaphore_signal(barrier, inc=1, device_id=dev, device_id_type=MESH)
    pl.semaphore_wait(barrier, len(peers))

    def product(start, count, cot, low, width):
        return lax.dot_general(
            x_ref[:, pl.ds(pl.multiple_of(start, 128), count)],
            cot[:, low : low + width],
            (((0,), (0,)), ((), ())),
            preferred_element_type=F32,
        )

    def add_a(chunk, half, recv):
        for y2 in range(2):
            def body(x2, _):
                at = (2 * half + y2, x2, chunk)
                ga[at] = ga[at] + recv[y2, x2]
                return 0
            lax.fori_loop(0, NX, body, 0)

    def add_b(chunk, half, recv):
        for y2 in range(2):
            def body(z2, _):
                at = (2 * half + y2, chunk, z2)
                gb[at] = gb[at] + recv[y2, z2]
                return 0
            lax.fori_loop(0, NZ, body, 0)

    def add_c(chunk, half, recv):
        for x2 in range(2):
            def body(z2, _):
                at = (chunk, 2 * half + x2, z2)
                gc[at] = gc[at] + recv[x2, z2]
                return 0
            lax.fori_loop(0, NZ, body, 0)

    ring_a = RingSum(net, Z, NZ, lambda c, h: ga.at[pl.ds(2 * h, 2), :, c], ra, add_a)
    ring_b = RingSum(net, X, NX, lambda c, h: gb.at[pl.ds(2 * h, 2), c], rb, add_b)
    ring_c = RingSum(net, Y, NY, lambda c, h: gc.at[c, pl.ds(2 * h, 2)], rc, add_c)

    def make_a(yy, _):
        ga[yy] = product(yy * 512, 512, qc_ref, 0, WA).reshape(NX, NZ, BLK, WA)
        return 0

    def make_b(chunk):
        def body(yy, _):
            gb[yy, chunk] = product(yy * 512 + chunk * 128, 128, qc_ref, WA, WB).reshape(NZ, BLK, WB)
            return 0
        lax.fori_loop(0, NY, body, 0)

    def make_c(chunk):
        gc[chunk, :, :, :, 0:128] = product(chunk * 512, 512, qc_ref, WA + WB, 128).reshape(NX, NZ, BLK, 128)
        gc[chunk, :, :, :, 128:WC] = product(chunk * 512, 512, kc_ref, 0, KN).reshape(NX, NZ, BLK, KN)

    lax.fori_loop(0, NY, make_a, 0)
    ring_a.send(0)
    ring_a.send(1)
    make_b(x_of[2])
    ring_b.send(0)
    make_c(y_of[2])
    ring_c.send(0)
    make_b(x_of[1])
    make_b(x_of[3])
    ring_b.send(1)
    make_c(y_of[1])
    make_c(y_of[3])
    ring_c.send(1)
    ring_a.send(2)
    make_b(x_of[0])
    make_c(y_of[0])

    roots[...] = jnp.zeros_like(roots)
    for p in range(PAIRS):
        ref, h = (qr_ref, 2 * p) if p < QPAIRS else (kr_ref, 2 * (p - QPAIRS))
        roots[p, 0:HEAD_DIM, 0:HEAD_DIM] = ref[h]
        roots[p, HEAD_DIM : 2 * HEAD_DIM, HEAD_DIM : 2 * HEAD_DIM] = ref[h + 1]

    ring_a.send(3)
    ring_b.send(2)
    ring_c.send(2)
    ring_a.send(4)
    ring_a.send(5)
    ring_a.send(6)

    ring_c.finish()
    to_c1 = [net.copy(gc.at[y, x_of[d]], c1.at[d - 1], {X: x_of[d]}) for d in (1, 3, 2)]
    start_all(to_c1)
    ring_b.finish()
    to_b1 = [net.copy(gb.at[y_of[d], x], b1.at[d - 1], {Y: y_of[d]}) for d in (1, 3, 2)]
    start_all(to_b1)

    wait_all(to_c1)
    def sum_c(zz, _):
        gc[y, x, zz] = (gc[y, x, zz] + c1[0, zz]) + (c1[1, zz] + c1[2, zz])
        return 0
    lax.fori_loop(0, NZ, sum_c, 0)
    to_c2 = [net.copy(gc.at[y, x, z_of[d]], c2.at[d - 1], {Z: z_of[d]}) for d in range(1, NZ)]
    start_all(to_c2)

    ring_a.finish()
    to_pa = [
        net.copy(ga.at[y_of[dy], x_of[dx], z], pa.at[i], {Y: y_of[dy], X: x_of[dx]})
        for i, (dy, dx) in enumerate(spots[1:])
    ]
    start_all(to_pa)

    wait_all(to_b1)
    def sum_b(zz, _):
        gb[y, x, zz] = (gb[y, x, zz] + b1[0, zz]) + (b1[1, zz] + b1[2, zz])
        return 0
    lax.fori_loop(0, NZ, sum_b, 0)
    to_b2 = [net.copy(gb.at[y, x, z_of[d]], b2.at[d - 1], {Z: z_of[d]}) for d in range(1, NZ)]
    start_all(to_b2)

    mine = gath.at[x, z]

    def settle(own, arrived, low, width):
        total = own
        for d in range(arrived.shape[0]):
            total = total + arrived[d]
        mine[:, low : low + width] = total.astype(BF16)

    wait_all(to_c2)
    settle(gc[y, x, z], c2, WA + WB, WC)
    wait_all(to_pa)
    settle(ga[y, x, z], pa, 0, WA)
    wait_all(to_b2)
    settle(gb[y, x, z], b2, WA, WB)

    p_x = [net.copy(gath.at[x, z, :, 0:WP], gath.at[x, z, :, 0:WP], {X: x_of[d]}, gath.at[x_of[NX - d], z, :, 0:WP]) for d in (1, 3, 2)]
    start_all(p_x)
    q_z = [net.copy(gath.at[x, z, :, WP:], gath.at[x, z, :, WP:], {Z: z_of[d]}, gath.at[x, z_of[NZ - d], :, WP:]) for d in (4, 3, 5, 2, 6, 1, 7)]
    start_all(q_z)
    ring_p = RingGather(net, Z, NZ, lambda c, h: [gath.at[pl.ds(2 * h, 2), c, :, 0:WP]])
    wait_all(p_x)
    ring_p.send(0)
    ring_p.send(1)
    wait_all(q_z)
    q_x = [net.copy(gath.at[x, :, :, WP:], gath.at[x, :, :, WP:], {X: x_of[d]}, gath.at[x_of[NX - d], :, :, WP:]) for d in (1, 3, 2)]
    start_all(q_x)
    for j in range(2, NZ - 1):
        ring_p.send(j)

    l_at = pl.ds(pl.multiple_of(y * 512, 512), 512)

    def tile(p):
        return gath[:, :, :, 128 * p : 128 * (p + 1)].reshape(NX * NZ * BLK, 128)

    def precondition(p):
        right = jnp.dot(tile(p), roots[p], preferred_element_type=F32).astype(BF16)
        left = ql_ref if p < QPAIRS else kl_ref
        part = jnp.dot(left[:, l_at], right, preferred_element_type=F32)
        pp[:, :, 128 * p : 128 * (p + 1)] = part.reshape(NY, BLK, 128)

    wait_all(q_x)
    for p in range(WP // 128, PAIRS):
        precondition(p)
    ring_p.finish()
    for p in range(WP // 128):
        precondition(p)

    to_pr = [net.copy(pp.at[y_of[d]], pr.at[d - 1], {Y: y_of[d]}) for d in (1, 3, 2)]
    start_all(to_pr)

    low_half = lax.broadcasted_iota(jnp.int32, (HEAD_DIM, 128), 1) < HEAD_DIM
    for p in range(PAIRS):
        both = lax.dot_general(tile(p), tile(p), (((0,), (0,)), ((), ())), preferred_element_type=F32)
        packed = jnp.where(low_half, both[0:HEAD_DIM], both[HEAD_DIM:])
        gp[:, p] = packed.reshape(NY, BLK, 128)

    rows = pl.ds(pl.multiple_of(y * BLK, BLK), BLK)
    wait_all(to_pr)
    pre = (pp[y] + pr[0]) + (pr[1] + pr[2])
    qm2 = MOMENT_DECAY * qm_ref[rows, :] + (1.0 - MOMENT_DECAY) * pre[:, :QN]
    km2 = MOMENT_DECAY * km_ref[rows, :] + (1.0 - MOMENT_DECAY) * pre[:, QN:]
    qw, kw = qw_ref[rows, :], kw_ref[rows, :]
    here = (y * NX + x) * NT + t
    plane[here] = jnp.concatenate(
        [lane_sums(v * v) for v in (qw, qm2, kw, km2)] + [jnp.zeros((4, 128), F32)], axis=0
    )
    mbuf[y, :, :QN] = qm2
    mbuf[y, :, QN:] = km2

    def slot_from(dy, dx, dt):
        return (y_of[(NY - dy) % NY] * NX + x_of[(NX - dx) % NX]) * NT + lax.rem(t + dt, NT)

    to_plane = [
        net.copy(
            plane.at[here], plane.at[here], {Y: y_of[dy], X: x_of[dx], T: lax.rem(t + dt, NT)},
            plane.at[slot_from(dy, dx, dt)],
        )
        for dy, dx, dt in others
    ]
    start_all(to_plane)
    to_m = [net.copy(mbuf.at[y], mbuf.at[y], {Y: y_of[d]}, mbuf.at[y_of[NY - d]]) for d in (1, 3, 2)]
    start_all(to_m)
    to_gr = [net.copy(gp.at[y_of[d]], gr.at[d - 1], {Y: y_of[d]}) for d in (1, 3, 2)]
    start_all(to_gr)
    wait_all(to_plane)
    total = plane[0]
    for i in range(1, NY * NX * NT):
        total = total + plane[i]
    zed[z] = total
    to_zed = [net.copy(zed.at[z], zed.at[z], {Z: z_of[d]}, zed.at[z_of[NZ - d]]) for d in (4, 3, 5, 2, 6, 1, 7)]
    start_all(to_zed)
    wait_all(to_zed)
    total = zed[0]
    for i in range(1, NZ):
        total = total + zed[i]
    total = jnp.sum(total, axis=1, keepdims=True)
    q_rate = LEARN_RATE * (jnp.sqrt(total[0:1]) / jnp.sqrt(total[1:2] + EPSILON))
    k_rate = LEARN_RATE * (jnp.sqrt(total[2:3]) / jnp.sqrt(total[3:4] + EPSILON))

    qcopy_ref[z, x, y] = (qw - q_rate * qm2).astype(BF16)
    kcopy_ref[z, x, y] = (kw - k_rate * km2).astype(BF16)

    def a_of(zi, xi, yi):
        return [qcopy_ref.at[zi, xi, yi, :, 0:WA]]

    def b_of(zi, xi, yi):
        return [qcopy_ref.at[zi, xi, yi, :, WA : WA + WB]]

    def c_of(zi, xi, yi):
        return [qcopy_ref.at[zi, xi, yi, :, WA + WB :], kcopy_ref.at[zi, xi, yi]]

    def spread(of, own, dev, source):
        return [net.copy(a, a, dev, b) for a, b in zip(of(*own), of(*source))]

    whole = slice(None)
    to_a, to_bz, to_cz, to_by, to_cx = [], [], [], [], []
    for dy, dx in spots[1:]:
        to_a += spread(a_of, (z, x, y), {Y: y_of[dy], X: x_of[dx]}, (z, x_of[(NX - dx) % NX], y_of[(NY - dy) % NY]))
    for d in (4, 3, 5, 2, 6, 1, 7):
        to_bz += spread(b_of, (z, x, y), {Z: z_of[d]}, (z_of[NZ - d], x, y))
        to_cz += spread(c_of, (z, x, y), {Z: z_of[d]}, (z_of[NZ - d], x, y))
    for d in (2, 1, 3):
        to_by += spread(b_of, (whole, x, y), {Y: y_of[d]}, (whole, x, y_of[NY - d]))
        to_cx += spread(c_of, (whole, x, y), {X: x_of[d]}, (whole, x_of[NX - d], y))
    ring_a = RingGather(net, Z, NZ, lambda c, h: a_of(c, pl.ds(2 * h, 2), whole))
    ring_b = RingGather(net, X, NX, lambda c, h: b_of(pl.ds(4 * h, 4), c, whole))
    ring_c = RingGather(net, Y, NY, lambda c, h: c_of(pl.ds(4 * h, 4), whole, c))

    start_all(to_a)
    start_all(to_bz)
    start_all(to_cz)
    wait_all(to_a)
    ring_a.send(0)
    ring_a.send(1)
    wait_all(to_bz)
    start_all(to_by)
    wait_all(to_cz)
    start_all(to_cx)

    wait_all(to_m)
    for yy in range(NY):
        at = slice(BLK * yy, BLK * (yy + 1))
        m = mbuf[yy, :, :QN]
        qm2_ref[at, :] = m
        qstep_ref[at, :] = q_rate * m
        qnext_ref[at, :] = qw_ref[at, :] - q_rate * m
        m = mbuf[yy, :, QN:]
        km2_ref[at, :] = m
        kstep_ref[at, :] = k_rate * m
        knext_ref[at, :] = kw_ref[at, :] - k_rate * m
    wait_all(to_gr)
    gfin[y] = (gp[y] + gr[0]) + (gr[1] + gr[2])
    to_gfin = [net.copy(gfin.at[y], gfin.at[y], {Y: y_of[d]}, gfin.at[y_of[NY - d]]) for d in (1, 3, 2)]

    ring_a.send(2)
    wait_all(to_by)
    ring_b.send(0)
    ring_b.send(1)
    ring_a.send(3)
    wait_all(to_cx)
    ring_c.send(0)
    ring_c.send(1)
    start_all(to_gfin)
    ring_a.send(4)
    ring_a.send(5)
    ring_b.send(2)
    ring_c.send(2)
    ring_a.send(6)

    wait_all(to_gfin)
    for p in range(PAIRS):
        source, target, h = (qs_ref, qs2_ref, 2 * p) if p < QPAIRS else (ks_ref, ks2_ref, 2 * (p - QPAIRS))
        gram = gfin[:, p].reshape(HEAD_DIM, 128) * ((1.0 - STAT_DECAY) / D)
        target[h] = STAT_DECAY * source[h] + gram[:, :HEAD_DIM]
        target[h + 1] = STAT_DECAY * source[h + 1] + gram[:, HEAD_DIM:]

    ring_b.finish()
    ring_c.finish()
    ring_a.finish()
    net.drain()


def shards(*args):
    space = pl.BlockSpec(memory_space=pltpu.VMEM)
    vm, dma = pltpu.VMEM, pltpu.SemaphoreType.DMA
    shape = jax.ShapeDtypeStruct
    blocks = (NZ, NX, NY, BLK)
    outs = pl.pallas_call(
        step_kernel,
        out_shape=(
            shape((64, QN), F32), shape((64, KN), F32),
            shape((64, QN), F32), shape((64, KN), F32),
            shape((*blocks, QN), BF16), shape((*blocks, KN), BF16),
            shape((64, QN), F32), shape((64, KN), F32),
            shape((16, 64, 64), F32), shape((4, 64, 64), F32),
        ),
        in_specs=[space] * 13,
        out_specs=[space] * 10,
        scratch_shapes=[
            vm((NY, NX, NZ, BLK, WA), F32),
            vm((NY, NX, NZ, BLK, WB), F32),
            vm((NY, NX, NZ, BLK, WC), F32),
            vm((2, 7, 2, NX, BLK, WA), F32),
            vm((2, 3, 2, NZ, BLK, WB), F32),
            vm((2, 3, 2, NZ, BLK, WC), F32),
            vm((15, BLK, WA), F32),
            vm((3, NZ, BLK, WB), F32),
            vm((3, NZ, BLK, WC), F32),
            vm((7, BLK, WB), F32),
            vm((7, BLK, WC), F32),
            vm((NX, NZ, BLK, QN + KN), BF16),
            vm((PAIRS, 128, 128), BF16),
            vm((NY, BLK, QN + KN), F32),
            vm((3, BLK, QN + KN), F32),
            vm((NY, BLK, QN + KN), F32),
            vm((NY, PAIRS, BLK, 128), F32),
            vm((3, PAIRS, BLK, 128), F32),
            vm((NY, PAIRS, BLK, 128), F32),
            vm((NY * NX * NT, 8, 128), F32),
            vm((NZ, 8, 128), F32),
            dma((COPIES,)),
            dma((COPIES,)),
        ],
        compiler_params=pltpu.CompilerParams(
            collective_id=0, has_side_effects=True, vmem_limit_bytes=62 * 2**20
        ),
        name="step",
    )(*args)
    outs = list(outs)
    outs[4] = outs[4].reshape(D, QN)
    outs[5] = outs[5].reshape(D, KN)
    return tuple(outs)


def solution(mesh):
    split = Mesh(mesh.devices.reshape(NZ, NX, NY, NT), (Z, X, Y, T))
    row = P(FS, T)
    head = P(T, None, None)
    whole = P(None, T)
    tok = P(FS_REP, T)
    return jax.shard_map(
        shards, mesh=split,
        in_specs=(P(FS_REP, None), tok, tok, row, row, row, row, P(FS, None), P(FS, None), head, head, head, head),
        out_specs=(row, row, row, row, whole, whole, row, row, head, head),
        check_vma=False,
    )
```

time: 569 us -> 156 us (0.27)
  waiting for transfers between devices: 450 us -> 0 us
  Pallas kernels: 67.2 us -> 140 us
  between operations: 16.7 us -> 0.68 us
  other arithmetic: 10.5 us -> 0 us
  starting transfers between devices: 7.7 us -> 0 us
  matrix products: 7.21 us -> 0 us
  local copies, waits for them, and re-layouts: 9.09 us -> 14.8 us
    all_gather x2 -> x0, waiting for transfers between devices: 230 us -> none  [the longest x1 116 us: shards(): copy = lax.all_gather(mine, FS_REP, axis=0, tiled=True)]
    psum x1 -> x0, waiting for transfers between devices: 213 us -> none  [shards(): gram = lax.psum(head_gram(rounded, root.shape[0]), ROWS)]
    pallas_call x1, Pallas kernels: 67.2 us -> 140 us  [shards(): pl.pallas_call(step_kernel, out_shape=(shape((64, QN), F32), shape((64, K...]
    unnamed x24 -> x20, local copies, waits for them, and re-layouts: 0.05 us -> 14.8 us
    all_to_all x1 -> x0, starting transfers between devices: 7.58 us -> none  [shards(): lax.all_to_all(jnp.broadcast_to(sums[None], (n, 4)), FS_TP, 0, 0, tiled=T...]
    slice x3 -> x0, local copies, waits for them, and re-layouts: 7.5 us -> none  [the longest x1 4.64 us: shards(): copy[:, :qn]]
    all_to_all x1 -> x0, waiting for transfers between devices: 7.3 us -> none  [shards(): lax.all_to_all(jnp.broadcast_to(sums[None], (n, 4)), FS_TP, 0, 0, tiled=T...]
    dot_general x4 -> x0, matrix products: 7.21 us -> none  [the longest x1 3.67 us: shards(): qp = jnp.dot(ql, piece[:, :qn], preferred_element_type=jnp.float32)]
  transfers between devices with their start and end apart: 4 -> 0, of which waited for: 4 -> 0; matrix products, arithmetic and copies ran while one was open for 2% -> 0% of each run, Pallas kernels for 0% -> 0%
where the time goes in v2:
time: 156 us; the launch traced here: 155 us
  Pallas kernels  140 us (90%)
  local copies, waits for them, and re-layouts  14.8 us (9%)
    pallas_call x1, Pallas kernels, shards(): pl.pallas_call(step_kernel, out_shape=(shape((64, QN), F32), shape((64, K...  140 us
    unnamed x20, local copies, waits for them, and re-layouts  14.8 us

profile of v2, /device:TPU:2, one launch (start us, length us, event | category | flops | bytes accessed | tf_op | source)
XLA Modules:
  0.0 155.4 jit_solution(8801798688837468378)
XLA Ops:
  0.6 139.9 %step.1 = (f32[64,1024]{1,0:T(8,128)}, f32[64,256]{1,0:T(8,128)}, f32[64,1024]{1,0:T(8,128)}, f32[64,256]{1,0:T(8,128)}, bf16[8,4,4,16,1024]{4,3,2,1,0:T(8,128)(...) custom-call(bf16[1024,2048]{1,0:T(8,128)(2,1)} %x_ref.1, ...), custom_call_target="tpu_custom_call" | custom-call | tf_op jit(solution)/shard_map/step/pallas_call | solution.py:462
  140.5 1.7 %copy.33 = f32[64,1024]{1,0:T(8,128)} copy(f32[64,1024]{1,0:T(8,128)} %get-tuple-element.40) | data formatting | bytes 524288
  142.2 1.5 copy.34
  143.7 1.7 %copy.35 = f32[64,1024]{1,0:T(8,128)} copy(f32[64,1024]{1,0:T(8,128)} %get-tuple-element.42) | data formatting | bytes 524288
  145.3 1.5 copy.36
  146.8 0.0 copy-start
  146.8 0.0 copy-start.2
  146.8 0.0 copy-start.4
  146.8 0.0 copy-start.1
  146.8 0.0 copy-start.3
  146.8 4.8 %copy.37 = bf16[2048,1024]{1,0:T(8,128)(2,1)} copy(bf16[2048,1024]{1,0:T(8,128)(2,1)} %bitcast.2) | data formatting | bytes 8388608
  151.6 0.0 copy-done
  151.6 1.0 copy.38
  152.6 0.0 copy-done.2
  152.6 0.7 copy.39
  153.3 0.0 copy-done.4
  153.3 0.6 copy.40
  153.9 0.0 copy-done.1
  153.9 0.8 copy.41
  154.7 0.0 copy-done.3
  154.7 0.7 copy.42
Async XLA Ops:
  146.8 4.8 %copy-start = (bf16[8,4,4,16,256]{4,3,2,1,0:T(8,128)(2,1)S(1)}, bf16[8,4,4,16,256]{4,3,2,1,0:T(8,128)(2,1)}, u32[]{:S(2)}) copy-start(bf16[8,4,4,16,256]{4,3,2,1,0:T(8,128)(2,1)} %get-tuple-element.25) | copy-start | bytes 3145732
  146.8 5.8 %copy-start.2 = (f32[64,1024]{1,0:T(8,128)S(1)}, f32[64,1024]{1,0:T(8,128)}, u32[]{:S(2)}) copy-start(f32[64,1024]{1,0:T(8,128)} %get-tuple-element.46) | copy-start | bytes 786436
  146.8 6.5 %copy-start.4 = (f32[64,256]{1,0:T(8,128)S(1)}, f32[64,256]{1,0:T(8,128)}, u32[]{:S(2)}) copy-start(f32[64,256]{1,0:T(8,128)} %get-tuple-element.47) | copy-start | bytes 196612
  146.8 7.1 %copy-start.1 = (f32[16,64,64]{2,1,0:T(8,128)S(1)}, f32[16,64,64]{2,1,0:T(8,128)}, u32[]{:S(2)}) copy-start(f32[16,64,64]{2,1,0:T(8,128)} %get-tuple-element.48) | copy-start | bytes 786436
  146.8 7.9 %copy-start.3 = (f32[4,64,64]{2,1,0:T(8,128)S(1)}, f32[4,64,64]{2,1,0:T(8,128)}, u32[]{:S(2)}) copy-start(f32[4,64,64]{2,1,0:T(8,128)} %get-tuple-element.49) | copy-start | bytes 196612

commit v3 on v2

--- a/solution.py
+++ b/solution.py
@@ -141,10 +141,12 @@
 
 
 def step_kernel(
-    x_ref, qc_ref, kc_ref, qw_ref, kw_ref, qm_ref, km_ref, ql_ref, kl_ref, qr_ref, kr_ref, qs_ref, ks_ref,
+    x_hbm, qc_hbm, kc_hbm, qw_hbm, kw_hbm, qm_hbm, km_hbm, ql_hbm, kl_hbm, qr_hbm, kr_hbm, qs_hbm, ks_hbm,
     qstep_ref, kstep_ref, qnext_ref, knext_ref, qcopy_ref, kcopy_ref, qm2_ref, km2_ref, qs2_ref, ks2_ref,
     ga, gb, gc, ra, rb, rc, pa, b1, c1, b2, c2,
-    gath, roots, pp, pr, mbuf, gp, gr, gfin, plane, zed, send_sem, recv_sem,
+    gath, roots, pp, pr, mbuf, gp, gr, gfin, plane, zed,
+    x_ref, qc_ref, kc_ref, qw_ref, kw_ref, qm_ref, km_ref, ql_ref, kl_ref, qr_ref, kr_ref, qs_ref, ks_ref,
+    send_sem, recv_sem, load_sem,
 ):
     z, x, y, t = (lax.axis_index(a) for a in (Z, X, Y, T))
     z_of = [lax.rem(z + d, NZ) for d in range(NZ)]
@@ -160,14 +162,20 @@
     barrier = pltpu.get_barrier_semaphore()
     for dev in peers:
         pl.semaphore_signal(barrier, inc=1, device_id=dev, device_id_type=MESH)
-    pl.semaphore_wait(barrier, len(peers))
-
-    def product(start, count, cot, low, width):
+
+    l_at = pl.ds(pl.multiple_of(y * 512, 512), 512)
+    loads = [(qc_hbm, qc_ref)]
+    loads += [(x_hbm.at[:, 512 * i : 512 * (i + 1)], x_ref.at[i]) for i in range(NY)]
+    loads += [(kc_hbm, kc_ref), (qr_hbm, qr_ref), (kr_hbm, kr_ref)]
+    loads += [(ql_hbm.at[:, l_at], ql_ref), (kl_hbm.at[:, l_at], kl_ref)]
+    loads += [(qw_hbm, qw_ref), (kw_hbm, kw_ref), (qm_hbm, qm_ref), (km_hbm, km_ref)]
+    loads += [(qs_hbm, qs_ref), (ks_hbm, ks_ref)]
+    loads = [pltpu.make_async_copy(a, b, load_sem.at[i]) for i, (a, b) in enumerate(loads)]
+    start_all(loads)
+
+    def product(rows, cot, low, width):
         return lax.dot_general(
-            x_ref[:, pl.ds(pl.multiple_of(start, 128), count)],
-            cot[:, low : low + width],
-            (((0,), (0,)), ((), ())),
-            preferred_element_type=F32,
+            rows, cot[:, low : low + width], (((0,), (0,)), ((), ())), preferred_element_type=F32
         )
 
     def add_a(chunk, half, recv):
@@ -198,25 +206,27 @@
     ring_b = RingSum(net, X, NX, lambda c, h: gb.at[pl.ds(2 * h, 2), c], rb, add_b)
     ring_c = RingSum(net, Y, NY, lambda c, h: gc.at[c, pl.ds(2 * h, 2)], rc, add_c)
 
-    def make_a(yy, _):
-        ga[yy] = product(yy * 512, 512, qc_ref, 0, WA).reshape(NX, NZ, BLK, WA)
-        return 0
-
     def make_b(chunk):
-        def body(yy, _):
-            gb[yy, chunk] = product(yy * 512 + chunk * 128, 128, qc_ref, WA, WB).reshape(NZ, BLK, WB)
-            return 0
-        lax.fori_loop(0, NY, body, 0)
+        at = pl.ds(pl.multiple_of(chunk * 128, 128), 128)
+        rows = jnp.concatenate([x_ref[i, :, at] for i in range(NY)], axis=1)
+        gb[:, chunk] = product(rows, qc_ref, WA, WB).reshape(NY, NZ, BLK, WB)
 
     def make_c(chunk):
-        gc[chunk, :, :, :, 0:128] = product(chunk * 512, 512, qc_ref, WA + WB, 128).reshape(NX, NZ, BLK, 128)
-        gc[chunk, :, :, :, 128:WC] = product(chunk * 512, 512, kc_ref, 0, KN).reshape(NX, NZ, BLK, KN)
-
-    lax.fori_loop(0, NY, make_a, 0)
+        rows = x_ref[chunk]
+        gc[chunk, :, :, :, 0:128] = product(rows, qc_ref, WA + WB, 128).reshape(NX, NZ, BLK, 128)
+        gc[chunk, :, :, :, 128:WC] = product(rows, kc_ref, 0, KN).reshape(NX, NZ, BLK, KN)
+
+    loads[0].wait()
+    for i in range(NY):
+        loads[1 + i].wait()
+        ga[i] = product(x_ref[i], qc_ref, 0, WA).reshape(NX, NZ, BLK, WA)
+    pl.semaphore_wait(barrier, len(peers))
     ring_a.send(0)
     ring_a.send(1)
     make_b(x_of[2])
     ring_b.send(0)
+    for load in loads[1 + NY :]:
+        load.wait()
     make_c(y_of[2])
     ring_c.send(0)
     make_b(x_of[1])
@@ -301,15 +311,13 @@
     for j in range(2, NZ - 1):
         ring_p.send(j)
 
-    l_at = pl.ds(pl.multiple_of(y * 512, 512), 512)
-
     def tile(p):
         return gath[:, :, :, 128 * p : 128 * (p + 1)].reshape(NX * NZ * BLK, 128)
 
     def precondition(p):
         right = jnp.dot(tile(p), roots[p], preferred_element_type=F32).astype(BF16)
         left = ql_ref if p < QPAIRS else kl_ref
-        part = jnp.dot(left[:, l_at], right, preferred_element_type=F32)
+        part = jnp.dot(left[...], right, preferred_element_type=F32)
         pp[:, :, 128 * p : 128 * (p + 1)] = part.reshape(NY, BLK, 128)
 
     wait_all(q_x)
@@ -454,21 +462,30 @@
     net.drain()
 
 
+def write_kernel(*refs):
+    n = len(refs) // 2
+    sem = refs[-1]
+    copies = [pltpu.make_async_copy(refs[i], refs[n + i], sem.at[i]) for i in range(n)]
+    start_all(copies)
+    wait_all(copies)
+
+
 def shards(*args):
+    hbm = pl.BlockSpec(memory_space=pltpu.HBM)
     space = pl.BlockSpec(memory_space=pltpu.VMEM)
     vm, dma = pltpu.VMEM, pltpu.SemaphoreType.DMA
-    shape = jax.ShapeDtypeStruct
     blocks = (NZ, NX, NY, BLK)
-    outs = pl.pallas_call(
+    outs = (
+        ((64, QN), F32), ((64, KN), F32),
+        ((64, QN), F32), ((64, KN), F32),
+        ((*blocks, QN), BF16), ((*blocks, KN), BF16),
+        ((64, QN), F32), ((64, KN), F32),
+        ((16, 64, 64), F32), ((4, 64, 64), F32),
+    )
+    results = pl.pallas_call(
         step_kernel,
-        out_shape=(
-            shape((64, QN), F32), shape((64, KN), F32),
-            shape((64, QN), F32), shape((64, KN), F32),
-            shape((*blocks, QN), BF16), shape((*blocks, KN), BF16),
-            shape((64, QN), F32), shape((64, KN), F32),
-            shape((16, 64, 64), F32), shape((4, 64, 64), F32),
-        ),
-        in_specs=[space] * 13,
+        out_shape=tuple(vm(*o) for o in outs),
+        in_specs=[hbm] * 13,
         out_specs=[space] * 10,
         scratch_shapes=[
             vm((NY, NX, NZ, BLK, WA), F32),
@@ -492,18 +509,31 @@
             vm((NY, PAIRS, BLK, 128), F32),
             vm((NY * NX * NT, 8, 128), F32),
             vm((NZ, 8, 128), F32),
+            vm((NY, 1024, 512), BF16), vm((1024, QN), BF16), vm((1024, KN), BF16),
+            vm((64, QN), F32), vm((64, KN), F32), vm((64, QN), F32), vm((64, KN), F32),
+            vm((64, 512), BF16), vm((64, 512), BF16),
+            vm((16, 64, 64), BF16), vm((4, 64, 64), BF16), vm((16, 64, 64), F32), vm((4, 64, 64), F32),
             dma((COPIES,)),
             dma((COPIES,)),
+            dma((16,)),
         ],
         compiler_params=pltpu.CompilerParams(
-            collective_id=0, has_side_effects=True, vmem_limit_bytes=62 * 2**20
+            collective_id=0, has_side_effects=True, vmem_limit_bytes=46 * 2**20
         ),
         name="step",
-    )(*args)
-    outs = list(outs)
-    outs[4] = outs[4].reshape(D, QN)
-    outs[5] = outs[5].reshape(D, KN)
-    return tuple(outs)
+    )(*(pltpu.with_memory_space_constraint(a, pltpu.HBM) for a in args))
+    written = list(pl.pallas_call(
+        write_kernel,
+        out_shape=tuple(jax.ShapeDtypeStruct(*o) for o in outs),
+        in_specs=[space] * 10,
+        out_specs=[hbm] * 10,
+        scratch_shapes=[dma((10,))],
+        compiler_params=pltpu.CompilerParams(vmem_limit_bytes=2**20),
+        name="write",
+    )(*(pltpu.with_memory_space_constraint(r, pltpu.VMEM) for r in results)))
+    written[4] = written[4].reshape(D, QN)
+    written[5] = written[5].reshape(D, KN)
+    return tuple(written)
 
 
 def solution(mesh):

time: 156 us -> 137 us (0.88)
  local copies, waits for them, and re-layouts: 14.8 us -> 0 us
  Pallas kernels: 140 us -> 135 us
    unnamed x20 -> x0, local copies, waits for them, and re-layouts: 14.8 us -> none
    pallas_call x1 -> x2, Pallas kernels: 140 us -> 135 us  [the longest x1 132 us: shards(): pl.pallas_call(step_kernel, out_shape=tuple((vm(*o) for o in outs)), in_s...]
where the time goes in v3:
time: 137 us; the launch traced here: 135 us
  Pallas kernels  135 us (99%)
    pallas_call x1, Pallas kernels, shards(): pl.pallas_call(step_kernel, out_shape=tuple((vm(*o) for o in outs)), in_s...  132 us
    pallas_call x1, Pallas kernels, shards(): pl.pallas_call(write_kernel, out_shape=tuple((jax.ShapeDtypeStruct(*o) fo...  2.92 us

profile of v3, /device:TPU:2, one launch (start us, length us, event | category | flops | bytes accessed | tf_op | source)
XLA Modules:
  0.0 135.3 jit_solution(16771905708890759696)
XLA Ops:
  0.6 131.7 %step.1 = (f32[64,1024]{1,0:T(8,128)S(1)}, f32[64,256]{1,0:T(8,128)S(1)}, f32[64,1024]{1,0:T(8,128)S(1)}, f32[64,256]{1,0:T(8,128)S(1)}, bf16[8,4,4,16,1024]{4,3...) custom-call(bf16[1024,2048]{1,0:T(8,128)(2,1)} %x_hbm.1, ...), custom_call_target="tpu_custom_call" | custom-call | tf_op jit(solution)/shard_map/step/pallas_call | solution.py:485
  132.4 2.9 %write.1 = (f32[64,1024]{1,0:T(8,128)}, f32[64,256]{1,0:T(8,128)}, f32[64,1024]{1,0:T(8,128)}, f32[64,256]{1,0:T(8,128)}, bf16[8,4,4,16,1024]{4,3,2,1,0:T(8,128)...) custom-call(f32[64,1024]{1,0:T(8,128)S(1)} %get-tuple-element.30.ref, ...), custom_call_target="tpu_custom_call" | custom-call | tf_op jit(solution)/shard_map/write/pallas_call | solution.py:525

commit v4 on v3

--- a/solution.py
+++ b/solution.py
@@ -19,11 +19,12 @@
 MESH = pl.DeviceIdType.MESH
 QN, KN = 1024, 256
 WA, WB, WC = 512, 384, 384
-WP = 640
+WP = 256
 BLK = 16
 PAIRS = 10
 QPAIRS = 8
-COPIES = 256
+COPIES = 288
+NEAR = (1, 7, 2, 6, 3, 5, 4)
 F32, BF16 = jnp.float32, jnp.bfloat16
 
 
@@ -153,6 +154,8 @@
     x_of = [lax.rem(x + d, NX) for d in range(NX)]
     y_of = [lax.rem(y + d, NY) for d in range(NY)]
     spots = [(dy, dx) for dy in range(NY) for dx in range(NX)]
+    spots.sort(key=lambda s: -min(s[0], NY - s[0]) - min(s[1], NX - s[1]))
+    spots = [(0, 0)] + spots[:-1]
     others = [(dy, dx, dt) for dy, dx in spots for dt in range(NT) if dy or dx or dt]
     net = Net(send_sem, recv_sem)
 
@@ -267,13 +270,6 @@
     to_c2 = [net.copy(gc.at[y, x, z_of[d]], c2.at[d - 1], {Z: z_of[d]}) for d in range(1, NZ)]
     start_all(to_c2)
 
-    ring_a.finish()
-    to_pa = [
-        net.copy(ga.at[y_of[dy], x_of[dx], z], pa.at[i], {Y: y_of[dy], X: x_of[dx]})
-        for i, (dy, dx) in enumerate(spots[1:])
-    ]
-    start_all(to_pa)
-
     wait_all(to_b1)
     def sum_b(zz, _):
         gb[y, x, zz] = (gb[y, x, zz] + b1[0, zz]) + (b1[1, zz] + b1[2, zz])
@@ -282,6 +278,13 @@
     to_b2 = [net.copy(gb.at[y, x, z_of[d]], b2.at[d - 1], {Z: z_of[d]}) for d in range(1, NZ)]
     start_all(to_b2)
 
+    ring_a.finish()
+    to_pa = [
+        net.copy(ga.at[y_of[dy], x_of[dx], z], pa.at[i], {Y: y_of[dy], X: x_of[dx]})
+        for i, (dy, dx) in enumerate(spots[1:])
+    ]
+    start_all(to_pa)
+
     mine = gath.at[x, z]
 
     def settle(own, arrived, low, width):
@@ -290,26 +293,57 @@
             total = total + arrived[d]
         mine[:, low : low + width] = total.astype(BF16)
 
+    def block(at, low, high):
+        return gath.at[at[0], at[1], :, low:high]
+
+    def same(at, low, high, dev, source):
+        held, coming = block(at, low, high), block(source, low, high)
+        return net.copy(held, held, dev, coming)
+
+    class Relay:
+        def __init__(self, low, high):
+            self.along_z = {d: same((x, z), low, high, {Z: z_of[d]}, (x, z_of[NZ - d])) for d in NEAR}
+            self.along_x = [same((x, z), low, high, {X: x_of[e]}, (x_of[NX - e], z)) for e in (2, 1, 3)]
+            self.on = {
+                d: [
+                    same((x, z_of[NZ - d]), low, high, {X: x_of[e]}, (x_of[NX - e], z_of[NZ - d]))
+                    for e in (2, 1, 3)
+                ]
+                for d in NEAR
+            }
+
+        def start(self):
+            start_all(self.along_z.values())
+            start_all(self.along_x)
+
+        def forward(self):
+            for d in NEAR:
+                self.along_z[d].wait()
+                start_all(self.on[d])
+
+        def finish(self):
+            wait_all(self.along_x)
+            for d in NEAR:
+                wait_all(self.on[d])
+
     wait_all(to_c2)
     settle(gc[y, x, z], c2, WA + WB, WC)
+    wait_all(to_b2)
+    settle(gb[y, x, z], b2, WA, WB)
+    relay_bc = Relay(WA, QN + KN)
+    relay_bc.start()
     wait_all(to_pa)
     settle(ga[y, x, z], pa, 0, WA)
-    wait_all(to_b2)
-    settle(gb[y, x, z], b2, WA, WB)
-
-    p_x = [net.copy(gath.at[x, z, :, 0:WP], gath.at[x, z, :, 0:WP], {X: x_of[d]}, gath.at[x_of[NX - d], z, :, 0:WP]) for d in (1, 3, 2)]
+    p_x = [same((x, z), 0, WP, {X: x_of[d]}, (x_of[NX - d], z)) for d in (2, 1, 3)]
     start_all(p_x)
-    q_z = [net.copy(gath.at[x, z, :, WP:], gath.at[x, z, :, WP:], {Z: z_of[d]}, gath.at[x, z_of[NZ - d], :, WP:]) for d in (4, 3, 5, 2, 6, 1, 7)]
-    start_all(q_z)
-    ring_p = RingGather(net, Z, NZ, lambda c, h: [gath.at[pl.ds(2 * h, 2), c, :, 0:WP]])
+    relay_a = Relay(WP, WA)
+    relay_a.start()
+    every = slice(None)
+    p_z = [same((every, z), 0, WP, {Z: z_of[d]}, (every, z_of[NZ - d])) for d in (4, 3, 5, 2, 6, 1, 7)]
+    relay_bc.forward()
     wait_all(p_x)
-    ring_p.send(0)
-    ring_p.send(1)
-    wait_all(q_z)
-    q_x = [net.copy(gath.at[x, :, :, WP:], gath.at[x, :, :, WP:], {X: x_of[d]}, gath.at[x_of[NX - d], :, :, WP:]) for d in (1, 3, 2)]
-    start_all(q_x)
-    for j in range(2, NZ - 1):
-        ring_p.send(j)
+    start_all(p_z)
+    relay_a.forward()
 
     def tile(p):
         return gath[:, :, :, 128 * p : 128 * (p + 1)].reshape(NX * NZ * BLK, 128)
@@ -320,15 +354,22 @@
         part = jnp.dot(left[...], right, preferred_element_type=F32)
         pp[:, :, 128 * p : 128 * (p + 1)] = part.reshape(NY, BLK, 128)
 
-    wait_all(q_x)
-    for p in range(WP // 128, PAIRS):
+    def to_owner(low, high):
+        copies = [
+            net.copy(pp.at[y_of[d], :, low:high], pr.at[d - 1, :, low:high], {Y: y_of[d]}) for d in (2, 1, 3)
+        ]
+        start_all(copies)
+        return copies
+
+    relay_bc.finish()
+    for p in range(WA // 128, PAIRS):
         precondition(p)
-    ring_p.finish()
-    for p in range(WP // 128):
+    to_pr = to_owner(WA, QN + KN)
+    relay_a.finish()
+    wait_all(p_z)
+    for p in range(WA // 128):
         precondition(p)
-
-    to_pr = [net.copy(pp.at[y_of[d]], pr.at[d - 1], {Y: y_of[d]}) for d in (1, 3, 2)]
-    start_all(to_pr)
+    to_pr += to_owner(0, WA)
 
     low_half = lax.broadcasted_iota(jnp.int32, (HEAD_DIM, 128), 1) < HEAD_DIM
     for p in range(PAIRS):

time: 137 us -> 131 us (0.956); the launches traced: 135 us -> 131 us
  Pallas kernels: 135 us -> 130 us
    pallas_call x1, Pallas kernels: 132 us -> 127 us  [shards(): pl.pallas_call(step_kernel, out_shape=tuple((vm(*o) for o in outs)), in_s...]
where the time goes in v4:
time: 131 us
  Pallas kernels  130 us (99%)
    pallas_call x1, Pallas kernels, shards(): pl.pallas_call(step_kernel, out_shape=tuple((vm(*o) for o in outs)), in_s...  127 us
    pallas_call x1, Pallas kernels, shards(): pl.pallas_call(write_kernel, out_shape=tuple((jax.ShapeDtypeStruct(*o) fo...  2.92 us

profile of v4, /device:TPU:2, one launch (start us, length us, event | category | flops | bytes accessed | tf_op | source)
XLA Modules:
  0.0 130.9 jit_solution(14336555448081008303)
XLA Ops:
  0.6 127.2 %step.1 = (f32[64,1024]{1,0:T(8,128)S(1)}, f32[64,256]{1,0:T(8,128)S(1)}, f32[64,1024]{1,0:T(8,128)S(1)}, f32[64,256]{1,0:T(8,128)S(1)}, bf16[8,4,4,16,1024]{4,3...) custom-call(bf16[1024,2048]{1,0:T(8,128)(2,1)} %x_hbm.1, ...), custom_call_target="tpu_custom_call" | custom-call | tf_op jit(solution)/shard_map/step/pallas_call | solution.py:526
  127.8 2.9 %write.1 = (f32[64,1024]{1,0:T(8,128)}, f32[64,256]{1,0:T(8,128)}, f32[64,1024]{1,0:T(8,128)}, f32[64,256]{1,0:T(8,128)}, bf16[8,4,4,16,1024]{4,3,2,1,0:T(8,128)...) custom-call(f32[64,1024]{1,0:T(8,128)S(1)} %get-tuple-element.30.ref, ...), custom_call_target="tpu_custom_call" | custom-call | tf_op jit(solution)/shard_map/write/pallas_call | solution.py:566

commit v5 on v4

--- a/solution.py
+++ b/solution.py
@@ -270,6 +270,13 @@
     to_c2 = [net.copy(gc.at[y, x, z_of[d]], c2.at[d - 1], {Z: z_of[d]}) for d in range(1, NZ)]
     start_all(to_c2)
 
+    ring_a.finish()
+    to_pa = [
+        net.copy(ga.at[y_of[dy], x_of[dx], z], pa.at[i], {Y: y_of[dy], X: x_of[dx]})
+        for i, (dy, dx) in enumerate(spots[1:])
+    ]
+    start_all(to_pa)
+
     wait_all(to_b1)
     def sum_b(zz, _):
         gb[y, x, zz] = (gb[y, x, zz] + b1[0, zz]) + (b1[1, zz] + b1[2, zz])
@@ -277,13 +284,6 @@
     lax.fori_loop(0, NZ, sum_b, 0)
     to_b2 = [net.copy(gb.at[y, x, z_of[d]], b2.at[d - 1], {Z: z_of[d]}) for d in range(1, NZ)]
     start_all(to_b2)
-
-    ring_a.finish()
-    to_pa = [
-        net.copy(ga.at[y_of[dy], x_of[dx], z], pa.at[i], {Y: y_of[dy], X: x_of[dx]})
-        for i, (dy, dx) in enumerate(spots[1:])
-    ]
-    start_all(to_pa)
 
     mine = gath.at[x, z]
 

time: 131 us -> 131 us (level)
  no operation moved by 1% of the time
where the time goes in v5:
time: 131 us
  Pallas kernels  130 us (99%)
    pallas_call x1, Pallas kernels, shards(): pl.pallas_call(step_kernel, out_shape=tuple((vm(*o) for o in outs)), in_s...  127 us
    pallas_call x1, Pallas kernels, shards(): pl.pallas_call(write_kernel, out_shape=tuple((jax.ShapeDtypeStruct(*o) fo...  2.92 us

profile of v5, /device:TPU:2, one launch (start us, length us, event | category | flops | bytes accessed | tf_op | source)
XLA Modules:
  0.0 130.7 jit_solution(7889990023265275618)
XLA Ops:
  0.6 127.0 %step.1 = (f32[64,1024]{1,0:T(8,128)S(1)}, f32[64,256]{1,0:T(8,128)S(1)}, f32[64,1024]{1,0:T(8,128)S(1)}, f32[64,256]{1,0:T(8,128)S(1)}, bf16[8,4,4,16,1024]{4,3...) custom-call(bf16[1024,2048]{1,0:T(8,128)(2,1)} %x_hbm.1, ...), custom_call_target="tpu_custom_call" | custom-call | tf_op jit(solution)/shard_map/step/pallas_call | solution.py:526
  127.6 2.9 %write.1 = (f32[64,1024]{1,0:T(8,128)}, f32[64,256]{1,0:T(8,128)}, f32[64,1024]{1,0:T(8,128)}, f32[64,256]{1,0:T(8,128)}, bf16[8,4,4,16,1024]{4,3,2,1,0:T(8,128)...) custom-call(f32[64,1024]{1,0:T(8,128)S(1)} %get-tuple-element.30.ref, ...), custom_call_target="tpu_custom_call" | custom-call | tf_op jit(solution)/shard_map/write/pallas_call | solution.py:566
